TPU v7x, 32 devices: a whole 2x2x4 slice. The times are simulated.
32 devices in a mesh: sp: 8 (over z, x), tp: 4 (over y, core).
Axes of the slice: x: 2, y: 2, z: 4, core: 2. Of those that a mesh axis runs over, the one named last changes fastest.
Arguments:
- query_maps: bfloat16 [1536, 1024], P('sp', 'tp'), may hold values from -6 to 6
- key_maps: bfloat16 [1536, 512], P('sp', 'tp'), may hold values from -6 to 6
- value_rows: bfloat16 [1536, 512], P('sp', 'tp'), may hold values from -6 to 6
- mix_lambda: float32 [8], P('tp'), may hold values from 0.3 to 0.8
- head_gain: float32 [128], replicated, may hold values from 0.1 to 1.9
- out_weight: bfloat16 [1024, 2048], replicated, may hold values from -0.1875 to 0.1875
- residual: bfloat16 [1536, 2048], P(('sp', 'tp')), may hold values from -6 to 6
- norm_gain: float32 [2048], replicated, may hold values from 0.1 to 1.9
- routes: int32 [1536, 4], P('sp'), may hold values from 0 to 7, all different within a row; in each aligned block of 48 rows (0 to 47, 48 to 95, ...) at most 48 rows name the same one
- route_weight: float32 [1536, 4], P(('sp', 'tp')), may hold values from 0.3 to 1.5
- expert_gate: bfloat16 [8, 2048, 1024], P('sp', None, 'tp'), may hold values from -0.125 to 0.125
- expert_up: bfloat16 [8, 2048, 1024], P('sp', None, 'tp'), may hold values from -0.125 to 0.125
- expert_down: bfloat16 [8, 1024, 2048], P('sp', 'tp'), may hold values from -0.1875 to 0.1875
- shared_gate: bfloat16 [2048, 1024], P(None, 'tp'), may hold values from -0.125 to 0.125
- shared_up: bfloat16 [2048, 1024], P(None, 'tp'), may hold values from -0.125 to 0.125
- shared_down: bfloat16 [1024, 2048], P('tp'), may hold values from -0.1875 to 0.1875
Outputs:
- mixed: bfloat16 [1536, 2048], P(('sp', 'tp'))
Inputs may be any that keep to these rules, and one draw needn't show every extreme that they name: `routes`: the 4 experts of a token are different. In each aligned block of 48 tokens (the tokens of one device after the attention) no expert is named more than 48 times, a bound that some expert reaches in some blocks.
All inputs are finite; a program needn't handle non-finite values.
Results may differ from a plain program's by a relative error of at most 0.018.
Values may be sent and summed in bfloat16 or wider, within the bound.
No kernel may reach another device: no remote copies, remote signals or barrier semaphores. Data moves between devices by JAX's collectives and lax.ppermute only.
A program may use at most 128 MiB of HBM per device.

v0:
```python
from functools import partial

import jax
import jax.numpy as jnp
from jax import lax
from jax.experimental import pallas as pl
from jax.experimental.pallas import tpu as pltpu
from jax.sharding import PartitionSpec as P

norm_eps = 1e-06
lowest_score = -1e30


def slot_targets(block_routes, experts, capacity):
    flat_routes = block_routes.reshape(-1)
    onehot = (flat_routes[:, None] == jnp.arange(experts, dtype=jnp.int32)[None, :]).astype(
        jnp.int32
    )
    earlier = jnp.cumsum(onehot, axis=0) - onehot
    return flat_routes * capacity + jnp.sum(earlier * onehot, axis=1)


def build_buffer(token_rows, block_routes, experts, capacity):
    targets = slot_targets(block_routes, experts, capacity)
    row_total = block_routes.shape[0]
    route_count = block_routes.shape[1]
    source_row = jnp.arange(row_total * route_count, dtype=jnp.int32) // route_count
    holder = jnp.full((experts * capacity,), row_total, jnp.int32).at[targets].set(source_row)
    padded = jnp.concatenate(
        [token_rows, jnp.zeros((1, token_rows.shape[1]), token_rows.dtype)], axis=0
    )
    return (padded[holder], targets)


def attention_block(carried, queries, key_block, value_block, score_scale):
    run_max, run_sum, accumulated = carried
    kv_local = run_max.shape[0]
    key_heads = key_block.reshape(key_block.shape[0], kv_local, 2, -1)
    value_heads = value_block.reshape(value_block.shape[0], kv_local, -1)
    scores = (
        jnp.einsum("qagcd,racd->agcqr", queries, key_heads, preferred_element_type=jnp.float32)
        * score_scale
    )
    new_max = jnp.maximum(run_max, jnp.max(scores, axis=-1))
    rescale = jnp.exp(run_max - new_max)
    weights = jnp.exp(scores - new_max[..., None])
    run_sum = run_sum * rescale + jnp.sum(weights, axis=-1)
    update = jnp.einsum(
        "agcqr,rae->agcqe",
        weights.astype(jnp.bfloat16),
        value_heads,
        preferred_element_type=jnp.float32,
    )
    return (new_max, run_sum, accumulated * rescale[..., None] + update)


def fold_keys(carried, pieces, first_row, queries, score_scale):
    key_piece, value_piece = pieces
    total_rows = key_piece.shape[0]
    block_rows = total_rows
    for candidate in (2048, 1024, 512):
        if total_rows % candidate == 0:
            block_rows = candidate
            break
    block_count = total_rows // block_rows

    def block_step(block_index, running):
        start_row = block_index * block_rows
        return attention_block(
            running,
            queries,
            lax.dynamic_slice_in_dim(key_piece, start_row, block_rows, 0),
            lax.dynamic_slice_in_dim(value_piece, start_row, block_rows, 0),
            score_scale,
        )

    return lax.fori_loop(0, block_count, block_step, carried)


def whole_experts(arrived, whole_gate, whole_up, whole_down, senders, capacity, groups):
    local_experts = whole_gate.shape[0]
    width = arrived.shape[-1]
    rows_in = arrived.reshape(senders, local_experts, capacity, width)
    gate_value = jnp.einsum(
        "sjtd,jdf->sjtf", rows_in, whole_gate, preferred_element_type=jnp.float32
    )
    up_value = jnp.einsum("sjtd,jdf->sjtf", rows_in, whole_up, preferred_element_type=jnp.float32)
    hidden = (jax.nn.silu(gate_value) * up_value).astype(jnp.bfloat16)
    hidden_units = hidden.shape[-1]
    hidden = hidden.reshape(senders, local_experts, capacity, groups, hidden_units // groups)
    down_groups = whole_down.reshape(local_experts, groups, hidden_units // groups, width)
    group_sums = jnp.einsum(
        "sjtgf,jgfd->sjtgd", hidden, down_groups, preferred_element_type=jnp.float32
    )
    group_sums = lax.optimization_barrier(group_sums.astype(jnp.bfloat16)).astype(jnp.float32)
    return (
        jnp.sum(group_sums, axis=3)
        .astype(jnp.bfloat16)
        .reshape(senders * local_experts * capacity, width)
    )


def exchange_body(
    query_maps,
    key_maps,
    value_rows,
    mix_lambda,
    head_gain,
    out_weight,
    residual,
    norm_gain,
    routes,
    route_weight,
    expert_gate,
    expert_up,
    expert_down,
    shared_gate,
    shared_up,
    shared_down,
):
    local_heads = mix_lambda.shape[0]
    head_width = head_gain.shape[0]
    kv_local = value_rows.shape[1] // head_width
    head_group = local_heads // kv_local
    head_dim = key_maps.shape[1] // (2 * kv_local)
    token_count = query_maps.shape[0]
    queries = query_maps.reshape(token_count, kv_local, head_group, 2, head_dim)
    start_max = jnp.full((kv_local, head_group, 2, token_count), lowest_score, jnp.float32)
    start_sum = jnp.zeros((kv_local, head_group, 2, token_count), jnp.float32)
    start_values = jnp.zeros((kv_local, head_group, 2, token_count, head_width), jnp.float32)
    folder = partial(fold_keys, queries=queries, score_scale=head_dim ** (-0.5))
    _, run_sum, accumulated = folder(
        (start_max, start_sum, start_values),
        (
            lax.all_gather(key_maps, "sp", axis=0, tiled=True),
            lax.all_gather(value_rows, "sp", axis=0, tiled=True),
        ),
        jnp.int32(0),
    )
    normalized = accumulated / run_sum[..., None]
    lambdas = mix_lambda.reshape(kv_local, head_group, 1, 1)
    difference = normalized[:, :, 0] - lambdas * normalized[:, :, 1]
    inverse_rms = lax.rsqrt(jnp.mean(difference * difference, axis=-1, keepdims=True) + norm_eps)
    head_scaled = (difference * inverse_rms * head_gain).astype(jnp.bfloat16)
    attended = jnp.transpose(head_scaled, (2, 0, 1, 3)).reshape(
        token_count, local_heads * head_width
    )
    columns = lax.axis_size("tp")
    column = lax.axis_index("tp")
    rows_dev = token_count // columns
    own_rows = lax.dynamic_slice_in_dim(
        out_weight, column * attended.shape[1], attended.shape[1], 0
    )
    projected = lax.psum_scatter(
        jnp.dot(attended, own_rows, preferred_element_type=jnp.float32).astype(jnp.bfloat16),
        "tp",
        scatter_dimension=0,
        tiled=True,
    ).astype(jnp.float32)
    stream = (residual.astype(jnp.float32) + projected).astype(jnp.bfloat16)
    stream_wide = stream.astype(jnp.float32)
    stream_rms = lax.rsqrt(jnp.mean(stream_wide * stream_wide, axis=1, keepdims=True) + norm_eps)
    normed = (stream_wide * stream_rms * norm_gain).astype(jnp.bfloat16)
    senders = lax.axis_size("sp")
    local_experts = expert_gate.shape[0]
    experts = senders * local_experts
    route_count = routes.shape[1]
    capacity = max(2, 2 * rows_dev * route_count // experts)
    local_routed = None
    whole_gate, whole_up, whole_down = (
        lax.all_gather(expert_gate, "tp", axis=2, tiled=True),
        lax.all_gather(expert_up, "tp", axis=2, tiled=True),
        lax.all_gather(expert_down, "tp", axis=1, tiled=True),
    )
    own_routes = lax.dynamic_slice_in_dim(routes, column * rows_dev, rows_dev, 0)
    buffer, targets = build_buffer(normed, own_routes, experts, capacity)
    arrived = lax.all_to_all(buffer, "sp", split_axis=0, concat_axis=0, tiled=True)
    local_routed = whole_experts(
        arrived, whole_gate, whole_up, whole_down, senders, capacity, columns
    )
    shared_rows = lax.all_gather(normed[None], "tp", axis=0, tiled=True)
    shared_in = shared_rows
    shared_in = shared_in.reshape(1 * lax.axis_size("tp") * rows_dev, shared_in.shape[-1])
    shared_hidden = (
        jax.nn.silu(jnp.dot(shared_in, shared_gate, preferred_element_type=jnp.float32))
        * jnp.dot(shared_in, shared_up, preferred_element_type=jnp.float32)
    ).astype(jnp.bfloat16)
    shared_out = jnp.dot(shared_hidden, shared_down, preferred_element_type=jnp.float32)
    pieces = shared_out.reshape(1 * lax.axis_size("tp"), rows_dev, shared_out.shape[-1])
    terms_out = pieces.astype(jnp.bfloat16)
    summed = (
        lax.psum_scatter(
            lax.optimization_barrier(terms_out).astype(jnp.float32).astype(jnp.bfloat16),
            "tp",
            scatter_dimension=0,
            tiled=True,
        )
        .astype(jnp.float32)[0]
        .astype(jnp.bfloat16)
    )
    returned = lax.all_to_all(local_routed, "sp", split_axis=0, concat_axis=0, tiled=True)
    picked = (
        returned[targets].reshape(rows_dev, route_count, returned.shape[-1]).astype(jnp.float32)
    )
    routed_sum = jnp.sum(route_weight[:, :, None] * picked, axis=1)
    return (stream_wide + summed.astype(jnp.float32) + routed_sum).astype(jnp.bfloat16)


def kernel_cost(flops):
    return pl.CostEstimate(flops=int(flops), transcendentals=0, bytes_accessed=0)


def vmem_mib(amount):
    return pltpu.CompilerParams(vmem_limit_bytes=amount * 2**20)


def whole_vmem(count):
    return [pl.BlockSpec(memory_space=pltpu.VMEM)] * count


def attention_kernel(place_ref, lambda_ref, query_ref, gain_ref, *refs, blocks, kv_local, score_scale):
    kv_refs, out_refs = refs[:blocks], refs[blocks:-2]
    kv_ref, held_ref = refs[-2:]
    rows, head_width = kv_refs[0].shape[0], gain_ref.shape[1]
    key_width = kv_refs[0].shape[1] - kv_local * head_width
    pair_width = key_width // kv_local
    head_group = query_ref.shape[1] // key_width
    for j in range(blocks):
        kv_ref[j * rows : (j + 1) * rows, :] = kv_refs[j][...]
    token_count = query_ref.shape[0]
    lane = lax.broadcasted_iota(jnp.int32, (token_count, pair_width), 1)
    factor = score_scale * 1.4426950408889634
    for g in range(kv_local):
        keys = kv_ref[:, g * pair_width : (g + 1) * pair_width]
        values = kv_ref[:, key_width + g * head_width : key_width + (g + 1) * head_width]
        for a in range(head_group):
            head = g * head_group + a
            both = query_ref[:, head * pair_width : (head + 1) * pair_width]
            parts = []
            for i in range(2):
                one = jnp.where((lane < pair_width // 2) == (i == 0), both, jnp.zeros_like(both))
                scores = lax.dot_general(
                    one, keys, (((1,), (1,)), ((), ())), preferred_element_type=jnp.float32
                )
                top = jnp.max(scores, axis=1, keepdims=True)
                weights = jnp.exp2((scores - top) * factor)
                total = jnp.sum(weights, axis=1, keepdims=True)
                parts.append(
                    jnp.dot(
                        weights.astype(jnp.bfloat16), values, preferred_element_type=jnp.float32
                    )
                    / total
                )
            difference = parts[0] - lambda_ref[head] * parts[1]
            mean = jnp.mean(difference * difference, axis=1, keepdims=True)
            held_ref[:, head * head_width : (head + 1) * head_width] = (
                difference * lax.rsqrt(mean + norm_eps) * gain_ref[...]
            ).astype(jnp.bfloat16)
    rows_dev = out_refs[0].shape[0]
    for step, out_ref in enumerate(out_refs):
        start = pl.multiple_of((place_ref[0] ^ step) * rows_dev, 16)
        out_ref[...] = held_ref[pl.ds(start, rows_dev), :]


def project_kernel(place_ref, weight_ref, residual_ref, gain_ref, marks_ref, *refs):
    part_refs, (stream_ref, packed_ref, slab_ref, sems) = refs[:-4], refs[-4:]
    width = residual_ref.shape[1]
    span = part_refs[0].shape[1]
    copies = []
    for step in range(len(part_refs)):
        start = pl.multiple_of((place_ref[0] ^ step) * span, span)
        copies.append(
            pltpu.make_async_copy(
                weight_ref.at[pl.ds(start, span), :], slab_ref.at[step], sems.at[step]
            )
        )
        copies[-1].start()
    total = residual_ref[...].astype(jnp.float32)
    for step, part_ref in enumerate(part_refs):
        copies[step].wait()
        total = total + jnp.dot(
            part_ref[...], slab_ref[step], preferred_element_type=jnp.float32
        )
    stream = total.astype(jnp.bfloat16)
    stream_ref[...] = stream
    wide = stream.astype(jnp.float32)
    rms = lax.rsqrt(jnp.mean(wide * wide, axis=1, keepdims=True) + norm_eps)
    packed_ref[:, :width] = (wide * rms * gain_ref[...]).astype(jnp.bfloat16)
    packed_ref[:, width:] = marks_ref[...]


def route_marks(routes, route_weight):
    lane = jnp.arange(128, dtype=jnp.int32)
    high = route_weight.astype(jnp.bfloat16).astype(jnp.float32)
    low = route_weight - high
    dense = jnp.zeros((routes.shape[0], 128), jnp.float32)
    for k in range(routes.shape[1]):
        route = routes[:, k : k + 1]
        dense = dense + jnp.where(lane == route, high[:, k : k + 1], 0.0)
        dense = dense + jnp.where(lane == route + 64, low[:, k : k + 1], 0.0)
    return dense.astype(jnp.bfloat16)


def expert_kernel(place_ref, *refs, pairs, weights, plain, shared, packed_own, packed_other):
    row_refs, refs = refs[: 2 * pairs], refs[2 * pairs :]
    near, out_refs = refs[:weights], refs[weights:]
    rows_dev, width = out_refs[0].shape
    rows = jnp.concatenate([ref[:, :width] for ref in row_refs], axis=0)
    marks = jnp.concatenate([ref[:, width:] for ref in row_refs], axis=0).astype(jnp.float32)
    lane = lax.broadcasted_iota(jnp.int32, marks.shape, 1)

    def weight_of(expert):
        chosen = jnp.logical_or(lane == expert, lane == expert + 64)
        return jnp.sum(jnp.where(chosen, marks, 0.0), axis=1, keepdims=True)

    own, other = weight_of(place_ref[1]), weight_of(place_ref[2])
    hiddens, downs = [], []
    at = 0
    for _ in range(plain):
        gate = jnp.dot(rows, near[at][...], preferred_element_type=jnp.float32)
        up = jnp.dot(rows, near[at + 1][...], preferred_element_type=jnp.float32)
        hiddens.append((jax.nn.silu(gate) * up * own).astype(jnp.bfloat16))
        downs.append(near[at + 2])
        at += 3
    for weight, count in ((own, packed_own), (other, packed_other)):
        for _ in range(count):
            pair = jnp.dot(rows, near[at][...], preferred_element_type=jnp.float32)
            units = pair.shape[1] // 2
            hidden = jax.nn.silu(pair[:, :units]) * pair[:, units:] * weight
            hiddens.append(hidden.astype(jnp.bfloat16))
            downs.append(near[at + 1])
            at += 2
    hidden = jnp.concatenate(hiddens, axis=1)
    common, common_downs = [], []
    for _ in range(shared):
        gate = jnp.dot(rows[: 2 * rows_dev], near[at][...], preferred_element_type=jnp.float32)
        up = jnp.dot(rows[: 2 * rows_dev], near[at + 1][...], preferred_element_type=jnp.float32)
        common.append((jax.nn.silu(gate) * up).astype(jnp.bfloat16))
        common_downs.append(near[at + 2])
        at += 3
    span = 256
    for start in range(0, width, span):
        columns = slice(start, start + span)
        down = jnp.concatenate([ref[:, columns] for ref in downs], axis=0)
        total = jnp.dot(hidden, down, preferred_element_type=jnp.float32)
        if shared:
            down = jnp.concatenate([ref[:, columns] for ref in common_downs], axis=0)
            extra = jnp.dot(
                jnp.concatenate(common, axis=1), down, preferred_element_type=jnp.float32
            )
        for j in range(2 * pairs):
            piece = total[j * rows_dev : (j + 1) * rows_dev]
            if shared and j < 2:
                piece = piece + extra[j * rows_dev : (j + 1) * rows_dev]
            out_refs[j][:, columns] = piece.astype(out_refs[j].dtype)


def run_copies(moves, sems):
    copies = [pltpu.make_async_copy(a, b, sems.at[i]) for i, (a, b) in enumerate(moves)]
    for copy in copies:
        copy.start()
    for copy in copies:
        copy.wait()


def join_kernel(key_ref, value_ref, out_ref, sems):
    width = key_ref.shape[1]
    run_copies(
        [(key_ref, out_ref.at[:, :width]), (value_ref, out_ref.at[:, width:])], sems
    )


def split_kernel(gate_ref, up_ref, down_ref, *refs):
    in_refs, out_refs, sems = refs[:2], refs[2:4], refs[4]
    half = gate_ref.shape[1] // 2
    moves = []
    for part in range(2):
        units = slice(part * half, (part + 1) * half)
        moves.append((gate_ref.at[:, units], in_refs[part].at[:, :half]))
        moves.append((up_ref.at[:, units], in_refs[part].at[:, half:]))
        moves.append((down_ref.at[units, :], out_refs[part]))
    run_copies(moves, sems)


def gathered_body(
    query_maps,
    key_maps,
    value_rows,
    mix_lambda,
    head_gain,
    out_weight,
    residual,
    norm_gain,
    routes,
    route_weight,
    expert_gate,
    expert_up,
    expert_down,
    shared_gate,
    shared_up,
    shared_down,
    *,
    senders,
    columns,
):
    def swap(value, sp_mask, tp_mask):
        pairs = [
            (s * columns + t, (s ^ sp_mask) * columns + (t ^ tp_mask))
            for s in range(senders)
            for t in range(columns)
        ]
        return lax.ppermute(value, ("sp", "tp"), pairs)

    def near(value):
        return pltpu.with_memory_space_constraint(value, pltpu.VMEM)

    def after(value, *others):
        return lax.optimization_barrier((value,) + others)[0]

    row = lax.axis_index("sp")
    column = lax.axis_index("tp")
    place = jnp.stack([column, row, row ^ 1]).astype(jnp.int32)
    rows_dev, width = residual.shape
    token_count = query_maps.shape[0]
    head_width = head_gain.shape[0]
    kv_local = value_rows.shape[1] // head_width
    head_dim = key_maps.shape[1] // (2 * kv_local)
    far = list(range(senders - 2, 0, -2))
    smem = pl.BlockSpec(memory_space=pltpu.SMEM)

    own_routes = lax.dynamic_slice_in_dim(routes, column * rows_dev, rows_dev, 0)
    marks = route_marks(own_routes, route_weight)

    anywhere = pl.BlockSpec(memory_space=pl.ANY)
    kv_own = pl.pallas_call(
        join_kernel,
        out_shape=pltpu.VMEM(
            (key_maps.shape[0], key_maps.shape[1] + value_rows.shape[1]), key_maps.dtype
        ),
        in_specs=[anywhere] * 2,
        out_specs=pl.BlockSpec(memory_space=pltpu.VMEM),
        scratch_shapes=[pltpu.SemaphoreType.DMA((2,))],
        compiler_params=vmem_mib(4),
        name="join",
    )(key_maps, value_rows)
    kv_line = [swap(kv_own, mask, 0) for mask in far]
    kv_side = [swap(block, 1, 0) for block in [kv_own] + kv_line]
    kv_blocks = [kv_own] + kv_line + kv_side
    query_maps, marks, place = lax.optimization_barrier((query_maps, marks, place))

    own_set = [expert_gate[0], expert_up[0], expert_down[0]]
    units = own_set[0].shape[1]
    half = units // 2
    pack_a, pack_b, down_a, down_b = pl.pallas_call(
        split_kernel,
        out_shape=[pltpu.VMEM((width, units), own_set[0].dtype)] * 2
        + [pltpu.VMEM((half, width), own_set[0].dtype)] * 2,
        in_specs=[anywhere] * 3,
        out_specs=whole_vmem(4),
        scratch_shapes=[pltpu.SemaphoreType.DMA((6,))],
        compiler_params=vmem_mib(4),
        name="split",
    )(*own_set)
    b_in, a_in = swap(pack_b, 0, 2), swap(pack_a, 1, 0)
    swapped = [swap(w, 0, 1) for w in own_set]
    shared_set = [shared_gate, shared_up, shared_down]
    shared_set = shared_set + [swap(w, 0, 1) for w in shared_set]

    kv_rows = sum(block.shape[0] for block in kv_blocks)
    head_columns = mix_lambda.shape[0] * head_width
    attended = pl.pallas_call(
        partial(
            attention_kernel,
            blocks=len(kv_blocks),
            kv_local=kv_local,
            score_scale=head_dim ** (-0.5),
        ),
        out_shape=[pltpu.VMEM((rows_dev, head_columns), jnp.bfloat16)] * columns,
        in_specs=[smem, smem] + whole_vmem(2 + len(kv_blocks)),
        out_specs=whole_vmem(columns),
        scratch_shapes=[
            pltpu.VMEM((kv_rows, kv_own.shape[1]), jnp.bfloat16),
            pltpu.VMEM((token_count, head_columns), jnp.bfloat16),
        ],
        cost_estimate=kernel_cost(4e9),
        compiler_params=vmem_mib(20),
        name="attention",
    )(place, mix_lambda, query_maps, head_gain[None], *map(near, kv_blocks))
    parts = [attended[0]] + [swap(attended[step], 0, step) for step in range(1, columns)]
    b_out, a_out = swap(down_b, 0, 2), swap(down_a, 1, 0)

    stream, packed = pl.pallas_call(
        project_kernel,
        out_shape=[
            pltpu.VMEM((rows_dev, width), jnp.bfloat16),
            pltpu.VMEM((rows_dev, width + 128), jnp.bfloat16),
        ],
        in_specs=[smem, pl.BlockSpec(memory_space=pl.ANY)] + whole_vmem(3 + columns),
        out_specs=whole_vmem(2),
        scratch_shapes=[
            pltpu.VMEM((columns, head_columns, width), jnp.bfloat16),
            pltpu.SemaphoreType.DMA((columns,)),
        ],
        cost_estimate=kernel_cost(2e9),
        compiler_params=vmem_mib(12),
        name="project",
    )(place, out_weight, residual, norm_gain[None], marks, *map(near, parts))

    line = [packed] + [swap(packed, mask, 0) for mask in far]
    side = [swap(block, 1, 2) for block in line]
    b_in, b_out = after((b_in, b_out), line[-1])
    a_in, a_out = after((a_in, a_out), line[-1])
    pack_set = [b_in, b_out, swap(b_in, 0, 1), swap(b_out, 0, 1)]
    pack_set += [a_in, a_out, swap(a_in, 0, 1), swap(a_out, 0, 1)]
    own_set = own_set + swapped

    def experts(chosen, with_shared):
        weights = own_set + pack_set + (shared_set if with_shared else [])
        rows = [block for i in chosen for block in (line[i], side[i])]
        kinds = [jnp.float32, jnp.bfloat16] * len(chosen)
        return pl.pallas_call(
            partial(
                expert_kernel,
                pairs=len(chosen),
                weights=len(weights),
                plain=2,
                shared=2 if with_shared else 0,
                packed_own=2,
                packed_other=2,
            ),
            out_shape=[pltpu.VMEM((rows_dev, width), kind) for kind in kinds],
            in_specs=[smem] + whole_vmem(len(rows) + len(weights)),
            out_specs=whole_vmem(len(kinds)),
            cost_estimate=kernel_cost(6e9),
            compiler_params=vmem_mib(20),
        name="experts",
        )(place, *map(near, rows), *map(near, weights))

    calls = [[0, 1], list(range(2, len(line)))] if len(line) > 2 else [list(range(len(line)))]
    masks = [0] + far
    total = stream.astype(jnp.float32)
    ready = None
    for number, chosen in enumerate(calls):
        if ready is not None:
            for i in chosen:
                line[i] = after(line[i], ready)
        outs = experts(chosen, number == 0)
        for spot in range(len(chosen) - 1, -1, -1):
            mask = masks[chosen[spot]]
            joined = outs[2 * spot] + swap(outs[2 * spot + 1], 1, 2).astype(jnp.float32)
            if mask:
                joined = joined.astype(jnp.bfloat16)
                ready = joined if ready is None else ready
                joined = swap(joined, mask, 0).astype(jnp.float32)
            total = total + joined
    return total.astype(jnp.bfloat16)


def body(*arguments, senders, columns):
    residual, routes, expert_gate = arguments[6], arguments[8], arguments[10]
    local_experts = expert_gate.shape[0]
    experts = senders * local_experts
    rows_dev, route_count = residual.shape[0], routes.shape[1]
    capacity = max(2, 2 * rows_dev * route_count // experts)
    paired = columns == 4 and senders > 1 and senders & (senders - 1) == 0
    if paired and local_experts == 1 and experts <= 64 and senders * rows_dev <= experts * capacity:
        return gathered_body(*arguments, senders=senders, columns=columns)
    return exchange_body(*arguments)


def solution(mesh):
    in_specs = (
        P("sp", "tp"),
        P("sp", "tp"),
        P("sp", "tp"),
        P("tp"),
        P(),
        P(),
        P(("sp", "tp"), None),
        P(),
        P("sp", None),
        P(("sp", "tp"), None),
        P("sp", None, "tp"),
        P("sp", None, "tp"),
        P("sp", "tp", None),
        P(None, "tp"),
        P(None, "tp"),
        P("tp", None),
    )
    out_specs = P(("sp", "tp"), None)
    return jax.shard_map(
        partial(body, senders=mesh.shape["sp"], columns=mesh.shape["tp"]), mesh=mesh, in_specs=in_specs, out_specs=out_specs, check_vma=False)
```

profile of v0, /device:TPU:0, one launch (start us, length us, event | category | flops | bytes accessed | tf_op | source)
XLA Modules:
  0.0 148.4 jit_solution(13235421662557778960)
XLA Ops:
  0.0 0.8 copy-done.4
  0.8 0.8 copy-done.5
  1.7 5.1 %collective-permute-start = (bf16[192,256]{1,0:T(8,128)(2,1)S(1)}, bf16[192,256]{1,0:T(8,128)(2,1)S(1)}, u32[]{:S(2)}, u32[]{:S(2)}) collective-permute-start(bf16[192,256]{1,0:T(8,128)(2,1)S(1)} %join.1.refs_0_), channel_id=1, source_target_pairs={{0,24},{1,25},{2,26},{3,27},{4,28},{5,29},{6,30},{7,31},{8,16},{9,... | collective-permute-start | bytes 294920 | tf_op jit(solution)/shard_map/ppermute | solution.py:412
  7.4 1.6 %collective-permute-start.3 = (bf16[192,256]{1,0:T(8,128)(2,1)S(1)}, bf16[192,256]{1,0:T(8,128)(2,1)S(1)}, u32[]{:S(2)}, u32[]{:S(2)}) collective-permute-start(bf16[192,256]{1,0:T(8,128)(2,1)S(1)} %join.1.refs_0_), channel_id=1, source_target_pairs={{0,4},{1,5},{2,6},{3,7},{4,0},{5,1},{6,2},{7,3},{8,12},{9,13},{10,... | collective-permute-start | bytes 294920 | tf_op jit(solution)/shard_map/ppermute | solution.py:412
  9.2 0.8 convert_convert_fusion
  10.5 1.5 %collective-permute-start.4 = (bf16[192,256]{1,0:T(8,128)(2,1)S(1)}, bf16[192,256]{1,0:T(8,128)(2,1)S(1)}, u32[]{:S(2)}, u32[]{:S(2)}) collective-permute-start(bf16[192,256]{1,0:T(8,128)(2,1)S(1)} %collective-permute-done.refs_1_), channel_id=1, source_target_pairs={{0,4},{1,5},{2,6},{3,7},{4,0},{5,1},{6,2},{7,3},{8,12},{9,13},{10,... | collective-permute-start | bytes 294920 | tf_op jit(solution)/shard_map/ppermute | solution.py:412
  12.0 3.1 %collective-permute-done.1.refs_2_ = bf16[192,256]{1,0:T(8,128)(2,1)S(1)} collective-permute-done((bf16[192,256]{1,0:T(8,128)(2,1)S(1)}, bf16[192,256]{1,0:T(8,128)(2,1)S(1)}, u32[]{:S(2)}, u32[]{:S(2)}) %collective-permute-start.1) | collective-permute-done | bytes 98336 | tf_op jit(solution)/shard_map/ppermute | solution.py:412
  15.1 1.5 %collective-permute-start.5 = (bf16[192,256]{1,0:T(8,128)(2,1)S(1)}, bf16[192,256]{1,0:T(8,128)(2,1)S(1)}, u32[]{:S(2)}, u32[]{:S(2)}) collective-permute-start(bf16[192,256]{1,0:T(8,128)(2,1)S(1)} %collective-permute-done.1.refs_2_), channel_id=1, source_target_pairs={{0,4},{1,5},{2,6},{3,7},{4,0},{5,1},{6,2},{7,3},{8,12},{9,13},{10,... | collective-permute-start | bytes 294920 | tf_op jit(solution)/shard_map/ppermute | solution.py:412
  17.2 3.0 %collective-permute-done.5.refs_6_ = bf16[192,256]{1,0:T(8,128)(2,1)S(1)} collective-permute-done((bf16[192,256]{1,0:T(8,128)(2,1)S(1)}, bf16[192,256]{1,0:T(8,128)(2,1)S(1)}, u32[]{:S(2)}, u32[]{:S(2)}) %collective-permute-start.5) | collective-permute-done | bytes 98336 | tf_op jit(solution)/shard_map/ppermute | solution.py:412
  20.2 1.1 collective-permute-done.6.refs_7_
  21.2 0.9 copy-done.11
  23.4 3.0 %attention.1 = (bf16[48,256]{1,0:T(8,128)(2,1)S(1)}, bf16[48,256]{1,0:T(8,128)(2,1)S(1)}, bf16[48,256]{1,0:T(8,128)(2,1)S(1)}, bf16[48,256]{1,0:T(8,128)(2,1)S(1)}) custom-call(s32[3]{0:T(128)S(1)} %pad_add_fusion.place_ref, f32[2]{0:T(128)S(1)} %copy-done.13, bf16[192,256]{1,0:T(8,128)(2,1)S(1)} %copy-done.11, f32[1,128]{1,0:T(1,128)S(1)} %bitcast.53, ...), custom_call_target="tpu_custom_call" | custom-call | flops 4000000000 | tf_op jit(solution)/shard_map/attention/pallas_call | solution.py:471
  26.5 1.6 %collective-permute-start.8 = (bf16[48,256]{1,0:T(8,128)(2,1)S(1)}, bf16[48,256]{1,0:T(8,128)(2,1)S(1)}, u32[]{:S(2)}, u32[]{:S(2)}) collective-permute-start(bf16[48,256]{1,0:T(8,128)(2,1)S(1)} %get-tuple-element.37), channel_id=1, source_target_pairs={{0,2},{1,3},{2,0},{3,1},{4,6},{5,7},{6,4},{7,5},{8,10},{9,11},{10,... | collective-permute-start | bytes 73736 | tf_op jit(solution)/shard_map/ppermute | solution.py:412
  28.4 2.0 %collective-permute-done.8.refs_2_ = bf16[48,256]{1,0:T(8,128)(2,1)S(1)} collective-permute-done((bf16[48,256]{1,0:T(8,128)(2,1)S(1)}, bf16[48,256]{1,0:T(8,128)(2,1)S(1)}, u32[]{:S(2)}, u32[]{:S(2)}) %collective-permute-start.8) | collective-permute-done | bytes 24608 | tf_op jit(solution)/shard_map/ppermute | solution.py:412
  30.4 1.0 collective-permute-done.9.refs_3_
  31.4 1.9 %project.1 = (bf16[48,2048]{1,0:T(8,128)(2,1)S(1)}, bf16[48,2176]{1,0:T(8,128)(2,1)S(1)}) custom-call(s32[3]{0:T(128)S(1)} %pad_add_fusion.place_ref, bf16[1024,2048]{1,0:T(8,128)(2,1)S(1)} %copy-done.6, bf16[48,2048]{1,0:T(8,128)(2,1)S(1)} %copy-done.10, f32[1,2048]{1,0:T(1,128)S(1)} %bitcast.52, bf16[48,128]{1,0:T(8,128)(2,1)S(1)} %add_convert_fusion.4.marks_ref, ...), custom_call_target="tpu_custom_call" | custom-call | flops 2000000000 | tf_op jit(solution)/shard_map/project/pallas_call | solution.py:492
  33.8 2.6 %collective-permute-start.11 = (bf16[48,2176]{1,0:T(8,128)(2,1)S(1)}, bf16[48,2176]{1,0:T(8,128)(2,1)S(1)}, u32[]{:S(2)}, u32[]{:S(2)}) collective-permute-start(bf16[48,2176]{1,0:T(8,128)(2,1)S(1)} %get-tuple-element.40.refs_0_), channel_id=1, source_target_pairs={{0,24},{1,25},{2,26},{3,27},{4,28},{5,29},{6,30},{7,31},{8,16},{9,... | collective-permute-start | bytes 626696 | tf_op jit(solution)/shard_map/ppermute | solution.py:412
  36.9 0.8 collective-permute-start.16
  37.8 1.2 collective-permute-start.17
  39.0 1.1 collective-permute-start.21
  40.6 1.4 collective-permute-start.22
  42.0 4.2 %collective-permute-done.11.refs_2_ = bf16[48,2176]{1,0:T(8,128)(2,1)S(1)} collective-permute-done((bf16[48,2176]{1,0:T(8,128)(2,1)S(1)}, bf16[48,2176]{1,0:T(8,128)(2,1)S(1)}, u32[]{:S(2)}, u32[]{:S(2)}) %collective-permute-start.11) | collective-permute-done | bytes 208928 | tf_op jit(solution)/shard_map/ppermute | solution.py:412
  46.2 1.2 collective-permute-start.10
  47.4 31.6 %collective-permute-done.10.refs_1_ = bf16[48,2176]{1,0:T(8,128)(2,1)S(1)} collective-permute-done((bf16[48,2176]{1,0:T(8,128)(2,1)S(1)}, bf16[48,2176]{1,0:T(8,128)(2,1)S(1)}, u32[]{:S(2)}, u32[]{:S(2)}) %collective-permute-start.10) | collective-permute-done | bytes 208928 | tf_op jit(solution)/shard_map/ppermute | solution.py:412
  79.0 1.8 %collective-permute-start.12 = (bf16[48,2176]{1,0:T(8,128)(2,1)S(1)}, bf16[48,2176]{1,0:T(8,128)(2,1)S(1)}, u32[]{:S(2)}, u32[]{:S(2)}) collective-permute-start(bf16[48,2176]{1,0:T(8,128)(2,1)S(1)} %collective-permute-done.11.refs_2_), channel_id=1, source_target_pairs={{0,6},{1,7},{2,4},{3,5},{4,2},{5,3},{6,0},{7,1},{8,14},{9,15},{10,... | collective-permute-start | bytes 626696 | tf_op jit(solution)/shard_map/ppermute | solution.py:412
  81.3 4.4 %collective-permute-done.12.refs_3_ = bf16[48,2176]{1,0:T(8,128)(2,1)S(1)} collective-permute-done((bf16[48,2176]{1,0:T(8,128)(2,1)S(1)}, bf16[48,2176]{1,0:T(8,128)(2,1)S(1)}, u32[]{:S(2)}, u32[]{:S(2)}) %collective-permute-start.12) | collective-permute-done | bytes 208928 | tf_op jit(solution)/shard_map/ppermute | solution.py:412
  86.8 1.5 %collective-permute-done.15.refs_9_ = bf16[256,2048]{1,0:T(8,128)(2,1)S(1)} collective-permute-done((bf16[256,2048]{1,0:T(8,128)(2,1)S(1)}, bf16[256,2048]{1,0:T(8,128)(2,1)S(1)}, u32[]{:S(2)}, u32[]{:S(2)}) %collective-permute-start.15) | collective-permute-done | bytes 1048608 | tf_op jit(solution)/shard_map/ppermute | solution.py:412
  88.5 1.4 collective-permute-done.25.refs_21_
  90.0 1.4 collective-permute-done.26.refs_22_
  91.5 1.4 collective-permute-done.27.refs_23_
  93.3 3.3 %collective-permute-done.20.refs_13_ = bf16[128,2048]{1,0:T(8,128)(2,1)S(1)} collective-permute-done((bf16[128,2048]{1,0:T(8,128)(2,1)S(1)}, bf16[128,2048]{1,0:T(8,128)(2,1)S(1)}, u32[]{:S(2)}, u32[]{:S(2)}) %collective-permute-start.20) | collective-permute-done | bytes 524320 | tf_op jit(solution)/shard_map/ppermute | solution.py:412
  96.6 0.7 collective-permute-done.24.refs_17_
  97.4 4.2 %experts.2 = (f32[48,2048]{1,0:T(8,128)S(1)}, bf16[48,2048]{1,0:T(8,128)(2,1)S(1)}, f32[48,2048]{1,0:T(8,128)S(1)}, bf16[48,2048]{1,0:T(8,128)(2,1)S(1)}) custom-call(s32[3]{0:T(128)S(1)} %pad_add_fusion.place_ref, bf16[48,2176]{1,0:T(8,128)(2,1)S(1)} %get-tuple-element.40.refs_0_, bf16[48,2176]{1,0:T(8,128)(2,1)S(1)} %collective-permute-done.10.refs_1_, ...), custom_call_target="tpu_custom_call" | custom-call | flops 6000000000 | tf_op jit(solution)/shard_map/experts/pallas_call | solution.py:521
  101.6 1.8 %collective-permute-start.28 = (bf16[48,2048]{1,0:T(8,128)(2,1)S(1)}, bf16[48,2048]{1,0:T(8,128)(2,1)S(1)}, u32[]{:S(2)}, u32[]{:S(2)}) collective-permute-start(bf16[48,2048]{1,0:T(8,128)(2,1)S(1)} %get-tuple-element.50), channel_id=1, source_target_pairs={{0,6},{1,7},{2,4},{3,5},{4,2},{5,3},{6,0},{7,1},{8,14},{9,15},{10,... | collective-permute-start | bytes 589832 | tf_op jit(solution)/shard_map/ppermute | solution.py:412
  103.5 1.1 collective-permute-start.33
  104.6 0.8 collective-permute-done.31.refs_0_
  105.4 1.8 %collective-permute-start.32 = (bf16[48,2176]{1,0:T(8,128)(2,1)S(1)}, bf16[48,2176]{1,0:T(8,128)(2,1)S(1)}, u32[]{:S(2)}, u32[]{:S(2)}) collective-permute-start(bf16[48,2176]{1,0:T(8,128)(2,1)S(1)} %collective-permute-done.31.refs_0_), channel_id=1, source_target_pairs={{0,6},{1,7},{2,4},{3,5},{4,2},{5,3},{6,0},{7,1},{8,14},{9,15},{10,... | collective-permute-start | bytes 626696 | tf_op jit(solution)/shard_map/ppermute | solution.py:412
  107.2 3.1 %collective-permute-done.28 = bf16[48,2048]{1,0:T(8,128)(2,1)S(1)} collective-permute-done((bf16[48,2048]{1,0:T(8,128)(2,1)S(1)}, bf16[48,2048]{1,0:T(8,128)(2,1)S(1)}, u32[]{:S(2)}, u32[]{:S(2)}) %collective-permute-start.28) | collective-permute-done | bytes 196640 | tf_op jit(solution)/shard_map/ppermute | solution.py:412
  110.4 8.1 %collective-permute-done.32.refs_1_ = bf16[48,2176]{1,0:T(8,128)(2,1)S(1)} collective-permute-done((bf16[48,2176]{1,0:T(8,128)(2,1)S(1)}, bf16[48,2176]{1,0:T(8,128)(2,1)S(1)}, u32[]{:S(2)}, u32[]{:S(2)}) %collective-permute-start.32) | collective-permute-done | bytes 208928 | tf_op jit(solution)/shard_map/ppermute | solution.py:412
  118.5 3.2 %experts.3 = (f32[48,2048]{1,0:T(8,128)S(1)}, bf16[48,2048]{1,0:T(8,128)(2,1)S(1)}, f32[48,2048]{1,0:T(8,128)S(1)}, bf16[48,2048]{1,0:T(8,128)(2,1)S(1)}) custom-call(s32[3]{0:T(128)S(1)} %pad_add_fusion.place_ref, bf16[48,2176]{1,0:T(8,128)(2,1)S(1)} %collective-permute-done.31.refs_0_, bf16[48,2176]{1,0:T(8,128)(2,1)S(1)} %collective-permute-done.32.refs_1_, ...), custom_call_target="tpu_custom_call" | custom-call | flops 6000000000 | tf_op jit(solution)/shard_map/experts/pallas_call | solution.py:521
  121.7 1.8 %collective-permute-start.34 = (bf16[48,2048]{1,0:T(8,128)(2,1)S(1)}, bf16[48,2048]{1,0:T(8,128)(2,1)S(1)}, u32[]{:S(2)}, u32[]{:S(2)}) collective-permute-start(bf16[48,2048]{1,0:T(8,128)(2,1)S(1)} %get-tuple-element.56), channel_id=1, source_target_pairs={{0,6},{1,7},{2,4},{3,5},{4,2},{5,3},{6,0},{7,1},{8,14},{9,15},{10,... | collective-permute-start | bytes 589832 | tf_op jit(solution)/shard_map/ppermute | solution.py:412
  123.5 1.1 collective-permute-start.30
  124.7 1.2 collective-permute-start.29
  125.9 2.0 %collective-permute-start.36 = (bf16[48,2048]{1,0:T(8,128)(2,1)S(1)}, bf16[48,2048]{1,0:T(8,128)(2,1)S(1)}, u32[]{:S(2)}, u32[]{:S(2)}) collective-permute-start(bf16[48,2048]{1,0:T(8,128)(2,1)S(1)} %get-tuple-element.58), channel_id=1, source_target_pairs={{0,6},{1,7},{2,4},{3,5},{4,2},{5,3},{6,0},{7,1},{8,14},{9,15},{10,... | collective-permute-start | bytes 589832 | tf_op jit(solution)/shard_map/ppermute | solution.py:412
  127.8 2.6 %collective-permute-done.34 = bf16[48,2048]{1,0:T(8,128)(2,1)S(1)} collective-permute-done((bf16[48,2048]{1,0:T(8,128)(2,1)S(1)}, bf16[48,2048]{1,0:T(8,128)(2,1)S(1)}, u32[]{:S(2)}, u32[]{:S(2)}) %collective-permute-start.34) | collective-permute-done | bytes 196640 | tf_op jit(solution)/shard_map/ppermute | solution.py:412
  131.1 6.0 %collective-permute-done.36 = bf16[48,2048]{1,0:T(8,128)(2,1)S(1)} collective-permute-done((bf16[48,2048]{1,0:T(8,128)(2,1)S(1)}, bf16[48,2048]{1,0:T(8,128)(2,1)S(1)}, u32[]{:S(2)}, u32[]{:S(2)}) %collective-permute-start.36) | collective-permute-done | bytes 196640 | tf_op jit(solution)/shard_map/ppermute | solution.py:412
  137.7 9.9 %collective-permute-done.37 = bf16[48,2048]{1,0:T(8,128)(2,1)S(1)} collective-permute-done((bf16[48,2048]{1,0:T(8,128)(2,1)S(1)}, bf16[48,2048]{1,0:T(8,128)(2,1)S(1)}, u32[]{:S(2)}, u32[]{:S(2)}) %collective-permute-start.37) | collective-permute-done | bytes 196640 | tf_op jit(solution)/shard_map/ppermute | solution.py:412
  147.6 0.8 add_convert_fusion
  (74 shorter events, 8.9 us)
Async XLA Ops:
  0.0 9.1 %copy-start = (s32[192,4]{0,1:T(4,128)S(1)}, s32[192,4]{0,1:T(4,128)}, u32[]{:S(2)}) copy-start(s32[192,4]{0,1:T(4,128)} %param.24) | copy-start | bytes 9220
  1.7 8.8 %collective-permute-start = (bf16[192,256]{1,0:T(8,128)(2,1)S(1)}, bf16[192,256]{1,0:T(8,128)(2,1)S(1)}, u32[]{:S(2)}, u32[]{:S(2)}) collective-permute-start(bf16[192,256]{1,0:T(8,128)(2,1)S(1)} %join.1.refs_0_), channel_id=1, source_target_pairs={{0,24},{1,25},{2,26},{3,27},{4,28},{5,29},{6,30},{7,31},{8,16},{9,... | collective-permute-start | bytes 294920 | tf_op jit(solution)/shard_map/ppermute | solution.py:412
  6.8 8.3 %collective-permute-start.1 = (bf16[192,256]{1,0:T(8,128)(2,1)S(1)}, bf16[192,256]{1,0:T(8,128)(2,1)S(1)}, u32[]{:S(2)}, u32[]{:S(2)}) collective-permute-start(bf16[192,256]{1,0:T(8,128)(2,1)S(1)} %join.1.refs_0_), channel_id=1, source_target_pairs={{0,16},{1,17},{2,18},{3,19},{4,20},{5,21},{6,22},{7,23},{8,24},{9,... | collective-permute-start | bytes 294920 | tf_op jit(solution)/shard_map/ppermute | solution.py:412
  6.8 9.8 %collective-permute-start.2 = (bf16[192,256]{1,0:T(8,128)(2,1)S(1)}, bf16[192,256]{1,0:T(8,128)(2,1)S(1)}, u32[]{:S(2)}, u32[]{:S(2)}) collective-permute-start(bf16[192,256]{1,0:T(8,128)(2,1)S(1)} %join.1.refs_0_), channel_id=1, source_target_pairs={{0,8},{1,9},{2,10},{3,11},{4,12},{5,13},{6,14},{7,15},{8,0},{9,1},... | collective-permute-start | bytes 294920 | tf_op jit(solution)/shard_map/ppermute | solution.py:412
  7.4 9.7 %collective-permute-start.3 = (bf16[192,256]{1,0:T(8,128)(2,1)S(1)}, bf16[192,256]{1,0:T(8,128)(2,1)S(1)}, u32[]{:S(2)}, u32[]{:S(2)}) collective-permute-start(bf16[192,256]{1,0:T(8,128)(2,1)S(1)} %join.1.refs_0_), channel_id=1, source_target_pairs={{0,4},{1,5},{2,6},{3,7},{4,0},{5,1},{6,2},{7,3},{8,12},{9,13},{10,... | collective-permute-start | bytes 294920 | tf_op jit(solution)/shard_map/ppermute | solution.py:412
  10.5 6.7 %collective-permute-start.4 = (bf16[192,256]{1,0:T(8,128)(2,1)S(1)}, bf16[192,256]{1,0:T(8,128)(2,1)S(1)}, u32[]{:S(2)}, u32[]{:S(2)}) collective-permute-start(bf16[192,256]{1,0:T(8,128)(2,1)S(1)} %collective-permute-done.refs_1_), channel_id=1, source_target_pairs={{0,4},{1,5},{2,6},{3,7},{4,0},{5,1},{6,2},{7,3},{8,12},{9,13},{10,... | collective-permute-start | bytes 294920 | tf_op jit(solution)/shard_map/ppermute | solution.py:412
  15.1 5.1 %collective-permute-start.5 = (bf16[192,256]{1,0:T(8,128)(2,1)S(1)}, bf16[192,256]{1,0:T(8,128)(2,1)S(1)}, u32[]{:S(2)}, u32[]{:S(2)}) collective-permute-start(bf16[192,256]{1,0:T(8,128)(2,1)S(1)} %collective-permute-done.1.refs_2_), channel_id=1, source_target_pairs={{0,4},{1,5},{2,6},{3,7},{4,0},{5,1},{6,2},{7,3},{8,12},{9,13},{10,... | collective-permute-start | bytes 294920 | tf_op jit(solution)/shard_map/ppermute | solution.py:412
  16.6 4.6 %collective-permute-start.6 = (bf16[192,256]{1,0:T(8,128)(2,1)S(1)}, bf16[192,256]{1,0:T(8,128)(2,1)S(1)}, u32[]{:S(2)}, u32[]{:S(2)}) collective-permute-start(bf16[192,256]{1,0:T(8,128)(2,1)S(1)} %collective-permute-done.2.refs_3_), channel_id=1, source_target_pairs={{0,4},{1,5},{2,6},{3,7},{4,0},{5,1},{6,2},{7,3},{8,12},{9,13},{10,... | collective-permute-start | bytes 294920 | tf_op jit(solution)/shard_map/ppermute | solution.py:412
  23.4 7.9 %copy-start.6 = (bf16[1024,2048]{1,0:T(8,128)(2,1)S(1)}, bf16[1024,2048]{1,0:T(8,128)(2,1)}, u32[]{:S(2)}) copy-start(bf16[1024,2048]{1,0:T(8,128)(2,1)} %weight_ref.1) | copy-start | bytes 12582916
  23.4 7.9 %copy-start.10 = (bf16[48,2048]{1,0:T(8,128)(2,1)S(1)}, bf16[48,2048]{1,0:T(8,128)(2,1)}, u32[]{:S(2)}) copy-start(bf16[48,2048]{1,0:T(8,128)(2,1)} %residual_ref.1) | copy-start | bytes 589828
  23.4 7.9 %copy-start.12 = (f32[2048]{0:T(1024)S(1)}, f32[2048]{0:T(1024)}, u32[]{:S(2)}) copy-start(f32[2048]{0:T(1024)} %param.23) | copy-start | bytes 24580
  26.4 10.0 %copy-start.1 = (bf16[1,2048,256]{2,1,0:T(8,128)(2,1)S(1)}, bf16[1,2048,256]{2,1,0:T(8,128)(2,1)}, u32[]{:S(2)}) copy-start(bf16[1,2048,256]{2,1,0:T(8,128)(2,1)} %param.26) | copy-start | bytes 3145732
  26.4 10.0 %copy-start.2 = (bf16[1,2048,256]{2,1,0:T(8,128)(2,1)S(1)}, bf16[1,2048,256]{2,1,0:T(8,128)(2,1)}, u32[]{:S(2)}) copy-start(bf16[1,2048,256]{2,1,0:T(8,128)(2,1)} %param.27) | copy-start | bytes 3145732
  26.4 10.0 %copy-start.3 = (bf16[1,256,2048]{2,1,0:T(8,128)(2,1)S(1)}, bf16[1,256,2048]{2,1,0:T(8,128)(2,1)}, u32[]{:S(2)}) copy-start(bf16[1,256,2048]{2,1,0:T(8,128)(2,1)} %param.28) | copy-start | bytes 3145732
  26.4 1.9 %collective-permute-start.7 = (bf16[48,256]{1,0:T(8,128)(2,1)S(1)}, bf16[48,256]{1,0:T(8,128)(2,1)S(1)}, u32[]{:S(2)}, u32[]{:S(2)}) collective-permute-start(bf16[48,256]{1,0:T(8,128)(2,1)S(1)} %get-tuple-element.36), channel_id=1, source_target_pairs={{0,1},{1,0},{2,3},{3,2},{4,5},{5,4},{6,7},{7,6},{8,9},{9,8},{10,11... | collective-permute-start | bytes 73736 | tf_op jit(solution)/shard_map/ppermute | solution.py:412
  26.5 3.9 %collective-permute-start.8 = (bf16[48,256]{1,0:T(8,128)(2,1)S(1)}, bf16[48,256]{1,0:T(8,128)(2,1)S(1)}, u32[]{:S(2)}, u32[]{:S(2)}) collective-permute-start(bf16[48,256]{1,0:T(8,128)(2,1)S(1)} %get-tuple-element.37), channel_id=1, source_target_pairs={{0,2},{1,3},{2,0},{3,1},{4,6},{5,7},{6,4},{7,5},{8,10},{9,11},{10,... | collective-permute-start | bytes 73736 | tf_op jit(solution)/shard_map/ppermute | solution.py:412
  28.1 3.3 %collective-permute-start.9 = (bf16[48,256]{1,0:T(8,128)(2,1)S(1)}, bf16[48,256]{1,0:T(8,128)(2,1)S(1)}, u32[]{:S(2)}, u32[]{:S(2)}) collective-permute-start(bf16[48,256]{1,0:T(8,128)(2,1)S(1)} %get-tuple-element.38), channel_id=1, source_target_pairs={{0,3},{1,2},{2,1},{3,0},{4,7},{5,6},{6,5},{7,4},{8,11},{9,10},{10,... | collective-permute-start | bytes 73736 | tf_op jit(solution)/shard_map/ppermute | solution.py:412
  31.4 54.3 %copy-start.7 = (bf16[2048,256]{1,0:T(8,128)(2,1)S(1)}, bf16[2048,256]{1,0:T(8,128)(2,1)}, u32[]{:S(2)}) copy-start(bf16[2048,256]{1,0:T(8,128)(2,1)} %refs_18_.1) | copy-start | bytes 3145732
  31.4 54.9 %copy-start.8 = (bf16[2048,256]{1,0:T(8,128)(2,1)S(1)}, bf16[2048,256]{1,0:T(8,128)(2,1)}, u32[]{:S(2)}) copy-start(bf16[2048,256]{1,0:T(8,128)(2,1)} %refs_19_.1) | copy-start | bytes 3145732
  31.4 54.9 %copy-start.9 = (bf16[256,2048]{1,0:T(8,128)(2,1)S(1)}, bf16[256,2048]{1,0:T(8,128)(2,1)}, u32[]{:S(2)}) copy-start(bf16[256,2048]{1,0:T(8,128)(2,1)} %refs_20_.1) | copy-start | bytes 3145732
  33.3 7.3 %collective-permute-start.18 = (bf16[48,2176]{1,0:T(8,128)(2,1)S(1)}, bf16[48,2176]{1,0:T(8,128)(2,1)S(1)}, u32[]{:S(2)}, u32[]{:S(2)}) collective-permute-start(bf16[48,2176]{1,0:T(8,128)(2,1)S(1)} %get-tuple-element.40.refs_0_), channel_id=1, source_target_pairs={{0,8},{1,9},{2,10},{3,11},{4,12},{5,13},{6,14},{7,15},{8,0},{9,1},... | collective-permute-start | bytes 626696 | tf_op jit(solution)/shard_map/ppermute | solution.py:412
  33.8 12.4 %collective-permute-start.11 = (bf16[48,2176]{1,0:T(8,128)(2,1)S(1)}, bf16[48,2176]{1,0:T(8,128)(2,1)S(1)}, u32[]{:S(2)}, u32[]{:S(2)}) collective-permute-start(bf16[48,2176]{1,0:T(8,128)(2,1)S(1)} %get-tuple-element.40.refs_0_), channel_id=1, source_target_pairs={{0,24},{1,25},{2,26},{3,27},{4,28},{5,29},{6,30},{7,31},{8,16},{9,... | collective-permute-start | bytes 626696 | tf_op jit(solution)/shard_map/ppermute | solution.py:412
  36.9 48.8 %collective-permute-start.16 = (bf16[2048,256]{1,0:T(8,128)(2,1)S(1)}, bf16[2048,256]{1,0:T(8,128)(2,1)S(1)}, u32[]{:S(2)}, u32[]{:S(2)}) collective-permute-start(bf16[2048,256]{1,0:T(8,128)(2,1)S(1)} %get-tuple-element.41), channel_id=1, source_target_pairs={{0,2},{1,3},{2,0},{3,1},{4,6},{5,7},{6,4},{7,5},{8,10},{9,11},{10,... | collective-permute-start | bytes 3145736 | tf_op jit(solution)/shard_map/ppermute | solution.py:412
  37.8 43.0 %collective-permute-start.17 = (bf16[128,2048]{1,0:T(8,128)(2,1)S(1)}, bf16[128,2048]{1,0:T(8,128)(2,1)S(1)}, u32[]{:S(2)}, u32[]{:S(2)}) collective-permute-start(bf16[128,2048]{1,0:T(8,128)(2,1)S(1)} %get-tuple-element.42), channel_id=1, source_target_pairs={{0,2},{1,3},{2,0},{3,1},{4,6},{5,7},{6,4},{7,5},{8,10},{9,11},{10,... | collective-permute-start | bytes 1572872 | tf_op jit(solution)/shard_map/ppermute | solution.py:412
  39.0 47.2 %collective-permute-start.21 = (bf16[2048,256]{1,0:T(8,128)(2,1)S(1)}, bf16[2048,256]{1,0:T(8,128)(2,1)S(1)}, u32[]{:S(2)}, u32[]{:S(2)}) collective-permute-start(bf16[2048,256]{1,0:T(8,128)(2,1)S(1)} %get-tuple-element.45), channel_id=1, source_target_pairs={{0,4},{1,5},{2,6},{3,7},{4,0},{5,1},{6,2},{7,3},{8,12},{9,13},{10,... | collective-permute-start | bytes 3145736 | tf_op jit(solution)/shard_map/ppermute | solution.py:412
  40.6 40.2 %collective-permute-start.22 = (bf16[128,2048]{1,0:T(8,128)(2,1)S(1)}, bf16[128,2048]{1,0:T(8,128)(2,1)S(1)}, u32[]{:S(2)}, u32[]{:S(2)}) collective-permute-start(bf16[128,2048]{1,0:T(8,128)(2,1)S(1)} %get-tuple-element.46), channel_id=1, source_target_pairs={{0,4},{1,5},{2,6},{3,7},{4,0},{5,1},{6,2},{7,3},{8,12},{9,13},{10,... | collective-permute-start | bytes 1572872 | tf_op jit(solution)/shard_map/ppermute | solution.py:412
  46.2 32.8 %collective-permute-start.10 = (bf16[48,2176]{1,0:T(8,128)(2,1)S(1)}, bf16[48,2176]{1,0:T(8,128)(2,1)S(1)}, u32[]{:S(2)}, u32[]{:S(2)}) collective-permute-start(bf16[48,2176]{1,0:T(8,128)(2,1)S(1)} %get-tuple-element.40.refs_0_), channel_id=1, source_target_pairs={{0,6},{1,7},{2,4},{3,5},{4,2},{5,3},{6,0},{7,1},{8,14},{9,15},{10,... | collective-permute-start | bytes 626696 | tf_op jit(solution)/shard_map/ppermute | solution.py:412
  79.0 6.7 %collective-permute-start.12 = (bf16[48,2176]{1,0:T(8,128)(2,1)S(1)}, bf16[48,2176]{1,0:T(8,128)(2,1)S(1)}, u32[]{:S(2)}, u32[]{:S(2)}) collective-permute-start(bf16[48,2176]{1,0:T(8,128)(2,1)S(1)} %collective-permute-done.11.refs_2_), channel_id=1, source_target_pairs={{0,6},{1,7},{2,4},{3,5},{4,2},{5,3},{6,0},{7,1},{8,14},{9,15},{10,... | collective-permute-start | bytes 626696 | tf_op jit(solution)/shard_map/ppermute | solution.py:412
  80.8 5.5 %collective-permute-start.13 = (bf16[2048,256]{1,0:T(8,128)(2,1)S(1)}, bf16[2048,256]{1,0:T(8,128)(2,1)S(1)}, u32[]{:S(2)}, u32[]{:S(2)}) collective-permute-start(bf16[2048,256]{1,0:T(8,128)(2,1)S(1)} %bitcast.41), channel_id=1, source_target_pairs={{0,1},{1,0},{2,3},{3,2},{4,5},{5,4},{6,7},{7,6},{8,9},{9,8},{10,11... | collective-permute-start | bytes 3145736 | tf_op jit(solution)/shard_map/ppermute | solution.py:412
  80.8 6.0 %collective-permute-start.14 = (bf16[2048,256]{1,0:T(8,128)(2,1)S(1)}, bf16[2048,256]{1,0:T(8,128)(2,1)S(1)}, u32[]{:S(2)}, u32[]{:S(2)}) collective-permute-start(bf16[2048,256]{1,0:T(8,128)(2,1)S(1)} %bitcast.45), channel_id=1, source_target_pairs={{0,1},{1,0},{2,3},{3,2},{4,5},{5,4},{6,7},{7,6},{8,9},{9,8},{10,11... | collective-permute-start | bytes 3145736 | tf_op jit(solution)/shard_map/ppermute | solution.py:412
  85.7 2.7 %collective-permute-start.15 = (bf16[256,2048]{1,0:T(8,128)(2,1)S(1)}, bf16[256,2048]{1,0:T(8,128)(2,1)S(1)}, u32[]{:S(2)}, u32[]{:S(2)}) collective-permute-start(bf16[256,2048]{1,0:T(8,128)(2,1)S(1)} %bitcast.49), channel_id=1, source_target_pairs={{0,1},{1,0},{2,3},{3,2},{4,5},{5,4},{6,7},{7,6},{8,9},{9,8},{10,11... | collective-permute-start | bytes 3145736 | tf_op jit(solution)/shard_map/ppermute | solution.py:412
  85.7 4.1 %collective-permute-start.25 = (bf16[2048,256]{1,0:T(8,128)(2,1)S(1)}, bf16[2048,256]{1,0:T(8,128)(2,1)S(1)}, u32[]{:S(2)}, u32[]{:S(2)}) collective-permute-start(bf16[2048,256]{1,0:T(8,128)(2,1)S(1)} %copy-done.7), channel_id=1, source_target_pairs={{0,1},{1,0},{2,3},{3,2},{4,5},{5,4},{6,7},{7,6},{8,9},{9,8},{10,11... | collective-permute-start | bytes 3145736 | tf_op jit(solution)/shard_map/ppermute | solution.py:412
  86.2 5.1 %collective-permute-start.26 = (bf16[2048,256]{1,0:T(8,128)(2,1)S(1)}, bf16[2048,256]{1,0:T(8,128)(2,1)S(1)}, u32[]{:S(2)}, u32[]{:S(2)}) collective-permute-start(bf16[2048,256]{1,0:T(8,128)(2,1)S(1)} %copy-done.8), channel_id=1, source_target_pairs={{0,1},{1,0},{2,3},{3,2},{4,5},{5,4},{6,7},{7,6},{8,9},{9,8},{10,11... | collective-permute-start | bytes 3145736 | tf_op jit(solution)/shard_map/ppermute | solution.py:412
  86.3 6.5 %collective-permute-start.27 = (bf16[256,2048]{1,0:T(8,128)(2,1)S(1)}, bf16[256,2048]{1,0:T(8,128)(2,1)S(1)}, u32[]{:S(2)}, u32[]{:S(2)}) collective-permute-start(bf16[256,2048]{1,0:T(8,128)(2,1)S(1)} %copy-done.9), channel_id=1, source_target_pairs={{0,1},{1,0},{2,3},{3,2},{4,5},{5,4},{6,7},{7,6},{8,9},{9,8},{10,11... | collective-permute-start | bytes 3145736 | tf_op jit(solution)/shard_map/ppermute | solution.py:412
  86.7 10.6 %collective-permute-start.19 = (bf16[2048,256]{1,0:T(8,128)(2,1)S(1)}, bf16[2048,256]{1,0:T(8,128)(2,1)S(1)}, u32[]{:S(2)}, u32[]{:S(2)}) collective-permute-start(bf16[2048,256]{1,0:T(8,128)(2,1)S(1)} %collective-permute-done.16.refs_10_), channel_id=1, source_target_pairs={{0,1},{1,0},{2,3},{3,2},{4,5},{5,4},{6,7},{7,6},{8,9},{9,8},{10,11... | collective-permute-start | bytes 3145736 | tf_op jit(solution)/shard_map/ppermute | solution.py:412
  88.4 9.0 %collective-permute-start.23 = (bf16[2048,256]{1,0:T(8,128)(2,1)S(1)}, bf16[2048,256]{1,0:T(8,128)(2,1)S(1)}, u32[]{:S(2)}, u32[]{:S(2)}) collective-permute-start(bf16[2048,256]{1,0:T(8,128)(2,1)S(1)} %collective-permute-done.21.refs_14_), channel_id=1, source_target_pairs={{0,1},{1,0},{2,3},{3,2},{4,5},{5,4},{6,7},{7,6},{8,9},{9,8},{10,11... | collective-permute-start | bytes 3145736 | tf_op jit(solution)/shard_map/ppermute | solution.py:412
  89.9 6.7 %collective-permute-start.20 = (bf16[128,2048]{1,0:T(8,128)(2,1)S(1)}, bf16[128,2048]{1,0:T(8,128)(2,1)S(1)}, u32[]{:S(2)}, u32[]{:S(2)}) collective-permute-start(bf16[128,2048]{1,0:T(8,128)(2,1)S(1)} %collective-permute-done.17.refs_11_), channel_id=1, source_target_pairs={{0,1},{1,0},{2,3},{3,2},{4,5},{5,4},{6,7},{7,6},{8,9},{9,8},{10,11... | collective-permute-start | bytes 1572872 | tf_op jit(solution)/shard_map/ppermute | solution.py:412
  91.4 6.0 %collective-permute-start.24 = (bf16[128,2048]{1,0:T(8,128)(2,1)S(1)}, bf16[128,2048]{1,0:T(8,128)(2,1)S(1)}, u32[]{:S(2)}, u32[]{:S(2)}) collective-permute-start(bf16[128,2048]{1,0:T(8,128)(2,1)S(1)} %collective-permute-done.22.refs_15_), channel_id=1, source_target_pairs={{0,1},{1,0},{2,3},{3,2},{4,5},{5,4},{6,7},{7,6},{8,9},{9,8},{10,11... | collective-permute-start | bytes 1572872 | tf_op jit(solution)/shard_map/ppermute | solution.py:412
  92.9 12.6 %collective-permute-start.31 = (bf16[48,2176]{1,0:T(8,128)(2,1)S(1)}, bf16[48,2176]{1,0:T(8,128)(2,1)S(1)}, u32[]{:S(2)}, u32[]{:S(2)}) collective-permute-start(bf16[48,2176]{1,0:T(8,128)(2,1)S(1)} %get-tuple-element.40.refs_0_), channel_id=1, source_target_pairs={{0,16},{1,17},{2,18},{3,19},{4,20},{5,21},{6,22},{7,23},{8,24},{9,... | collective-permute-start | bytes 626696 | tf_op jit(solution)/shard_map/ppermute | solution.py:412
  101.6 8.7 %collective-permute-start.28 = (bf16[48,2048]{1,0:T(8,128)(2,1)S(1)}, bf16[48,2048]{1,0:T(8,128)(2,1)S(1)}, u32[]{:S(2)}, u32[]{:S(2)}) collective-permute-start(bf16[48,2048]{1,0:T(8,128)(2,1)S(1)} %get-tuple-element.50), channel_id=1, source_target_pairs={{0,6},{1,7},{2,4},{3,5},{4,2},{5,3},{6,0},{7,1},{8,14},{9,15},{10,... | collective-permute-start | bytes 589832 | tf_op jit(solution)/shard_map/ppermute | solution.py:412
  103.5 15.0 %collective-permute-start.33 = (bf16[48,2176]{1,0:T(8,128)(2,1)S(1)}, bf16[48,2176]{1,0:T(8,128)(2,1)S(1)}, u32[]{:S(2)}, u32[]{:S(2)}) collective-permute-start(bf16[48,2176]{1,0:T(8,128)(2,1)S(1)} %collective-permute-done.18.refs_2_), channel_id=1, source_target_pairs={{0,6},{1,7},{2,4},{3,5},{4,2},{5,3},{6,0},{7,1},{8,14},{9,15},{10,... | collective-permute-start | bytes 626696 | tf_op jit(solution)/shard_map/ppermute | solution.py:412
  105.4 13.0 %collective-permute-start.32 = (bf16[48,2176]{1,0:T(8,128)(2,1)S(1)}, bf16[48,2176]{1,0:T(8,128)(2,1)S(1)}, u32[]{:S(2)}, u32[]{:S(2)}) collective-permute-start(bf16[48,2176]{1,0:T(8,128)(2,1)S(1)} %collective-permute-done.31.refs_0_), channel_id=1, source_target_pairs={{0,6},{1,7},{2,4},{3,5},{4,2},{5,3},{6,0},{7,1},{8,14},{9,15},{10,... | collective-permute-start | bytes 626696 | tf_op jit(solution)/shard_map/ppermute | solution.py:412
  121.7 8.7 %collective-permute-start.34 = (bf16[48,2048]{1,0:T(8,128)(2,1)S(1)}, bf16[48,2048]{1,0:T(8,128)(2,1)S(1)}, u32[]{:S(2)}, u32[]{:S(2)}) collective-permute-start(bf16[48,2048]{1,0:T(8,128)(2,1)S(1)} %get-tuple-element.56), channel_id=1, source_target_pairs={{0,6},{1,7},{2,4},{3,5},{4,2},{5,3},{6,0},{7,1},{8,14},{9,15},{10,... | collective-permute-start | bytes 589832 | tf_op jit(solution)/shard_map/ppermute | solution.py:412
  123.5 14.2 %collective-permute-start.30 = (bf16[48,2048]{1,0:T(8,128)(2,1)S(1)}, bf16[48,2048]{1,0:T(8,128)(2,1)S(1)}, u32[]{:S(2)}, u32[]{:S(2)}) collective-permute-start(bf16[48,2048]{1,0:T(8,128)(2,1)S(1)} %get-tuple-element.52), channel_id=1, source_target_pairs={{0,6},{1,7},{2,4},{3,5},{4,2},{5,3},{6,0},{7,1},{8,14},{9,15},{10,... | collective-permute-start | bytes 589832 | tf_op jit(solution)/shard_map/ppermute | solution.py:412
  124.7 13.0 %collective-permute-start.29 = (bf16[48,2048]{1,0:T(8,128)(2,1)S(1)}, bf16[48,2048]{1,0:T(8,128)(2,1)S(1)}, u32[]{:S(2)}, u32[]{:S(2)}) collective-permute-start(bf16[48,2048]{1,0:T(8,128)(2,1)S(1)} %add_convert_fusion.3), channel_id=1, source_target_pairs={{0,24},{1,25},{2,26},{3,27},{4,28},{5,29},{6,30},{7,31},{8,16},{9,... | collective-permute-start | bytes 589832 | tf_op jit(solution)/shard_map/ppermute | solution.py:412
  125.9 11.3 %collective-permute-start.36 = (bf16[48,2048]{1,0:T(8,128)(2,1)S(1)}, bf16[48,2048]{1,0:T(8,128)(2,1)S(1)}, u32[]{:S(2)}, u32[]{:S(2)}) collective-permute-start(bf16[48,2048]{1,0:T(8,128)(2,1)S(1)} %get-tuple-element.58), channel_id=1, source_target_pairs={{0,6},{1,7},{2,4},{3,5},{4,2},{5,3},{6,0},{7,1},{8,14},{9,15},{10,... | collective-permute-start | bytes 589832 | tf_op jit(solution)/shard_map/ppermute | solution.py:412
  130.5 7.2 %collective-permute-start.35 = (bf16[48,2048]{1,0:T(8,128)(2,1)S(1)}, bf16[48,2048]{1,0:T(8,128)(2,1)S(1)}, u32[]{:S(2)}, u32[]{:S(2)}) collective-permute-start(bf16[48,2048]{1,0:T(8,128)(2,1)S(1)} %add_convert_fusion.2), channel_id=1, source_target_pairs={{0,8},{1,9},{2,10},{3,11},{4,12},{5,13},{6,14},{7,15},{8,0},{9,1},... | collective-permute-start | bytes 589832 | tf_op jit(solution)/shard_map/ppermute | solution.py:412
  137.2 10.4 %collective-permute-start.37 = (bf16[48,2048]{1,0:T(8,128)(2,1)S(1)}, bf16[48,2048]{1,0:T(8,128)(2,1)S(1)}, u32[]{:S(2)}, u32[]{:S(2)}) collective-permute-start(bf16[48,2048]{1,0:T(8,128)(2,1)S(1)} %add_convert_fusion.1), channel_id=1, source_target_pairs={{0,16},{1,17},{2,18},{3,19},{4,20},{5,21},{6,22},{7,23},{8,24},{9,... | collective-permute-start | bytes 589832 | tf_op jit(solution)/shard_map/ppermute | solution.py:412
  (5 other events, 3.8 us)
where the time goes:
time: 149 us; the launch traced here: 148 us
  waiting for transfers between devices  91.4 us (61%)
  starting transfers between devices  38 us (26%)
  Pallas kernels  12.8 us (9%)
  local copies, waits for them, and re-layouts  3.94 us (3%)
  other arithmetic  1.99 us (1%)
    ppermute x38, waiting for transfers between devices, swap(): return lax.ppermute(value, ('sp', 'tp'), pairs)  91.4 us
    ppermute x38, starting transfers between devices, swap(): return lax.ppermute(value, ('sp', 'tp'), pairs)  38 us
    pallas_call x2, Pallas kernels, experts(): pl.pallas_call(partial(expert_kernel, pairs=len(chosen), weights=len(weig...  7.43 us
    unnamed x30, local copies, waits for them, and re-layouts  3.86 us
  transfers between devices with their start and end apart: 38, of which 22 were waited for; matrix products, arithmetic and copies ran while one was open for 1% of the time, Pallas kernels for 3%

commit v1 on v0

--- a/solution.py
+++ b/solution.py
@@ -251,7 +251,7 @@
                     )
                     / total
                 )
-            difference = parts[0] - lambda_ref[head] * parts[1]
+            difference = parts[0] - lambda_ref[:, head : head + 1] * parts[1]
             mean = jnp.mean(difference * difference, axis=1, keepdims=True)
             held_ref[:, head * head_width : (head + 1) * head_width] = (
                 difference * lax.rsqrt(mean + norm_eps) * gain_ref[...]
@@ -289,15 +289,23 @@
     packed_ref[:, width:] = marks_ref[...]
 
 
-def route_marks(routes, route_weight):
-    lane = jnp.arange(128, dtype=jnp.int32)
-    high = route_weight.astype(jnp.bfloat16).astype(jnp.float32)
-    low = route_weight - high
-    dense = jnp.zeros((routes.shape[0], 128), jnp.float32)
-    for k in range(routes.shape[1]):
-        route = routes[:, k : k + 1]
-        dense = dense + jnp.where(lane == route, high[:, k : k + 1], 0.0)
-        dense = dense + jnp.where(lane == route + 64, low[:, k : k + 1], 0.0)
+def route_marks(place_ref, routes_ref, weight_ref):
+    rows_dev = weight_ref.shape[1]
+    wide = (rows_dev, routes_ref.shape[1])
+    token = lax.broadcasted_iota(jnp.int32, wide, 0) + place_ref[0] * rows_dev
+    chosen = token == lax.broadcasted_iota(jnp.int32, wide, 1)
+    square = (rows_dev, rows_dev)
+    same = lax.broadcasted_iota(jnp.int32, square, 0) == lax.broadcasted_iota(jnp.int32, square, 1)
+    lane = lax.broadcasted_iota(jnp.int32, (rows_dev, 128), 1)
+    dense = jnp.zeros((rows_dev, 128), jnp.float32)
+    for k in range(routes_ref.shape[0]):
+        named = jnp.where(chosen, routes_ref[k : k + 1, :].astype(jnp.float32), 0.0)
+        route = jnp.sum(named, axis=1, keepdims=True).astype(jnp.int32)
+        held = jnp.where(same, weight_ref[k : k + 1, :], 0.0)
+        weight = jnp.sum(held, axis=1, keepdims=True)
+        high = weight.astype(jnp.bfloat16).astype(jnp.float32)
+        dense = dense + jnp.where(lane == route, high, 0.0)
+        dense = dense + jnp.where(lane == route + 64, weight - high, 0.0)
     return dense.astype(jnp.bfloat16)
 
 
@@ -322,14 +330,15 @@
         hiddens.append((jax.nn.silu(gate) * up * own).astype(jnp.bfloat16))
         downs.append(near[at + 2])
         at += 3
-    for weight, count in ((own, packed_own), (other, packed_other)):
-        for _ in range(count):
-            pair = jnp.dot(rows, near[at][...], preferred_element_type=jnp.float32)
+    for weight, pieces in ((own, packed_own), (other, packed_other)):
+        for _ in range(2):
+            whole = jnp.concatenate([near[at + i][...] for i in range(pieces)], axis=0)
+            pair = jnp.dot(rows, whole, preferred_element_type=jnp.float32)
             units = pair.shape[1] // 2
             hidden = jax.nn.silu(pair[:, :units]) * pair[:, units:] * weight
             hiddens.append(hidden.astype(jnp.bfloat16))
-            downs.append(near[at + 1])
-            at += 2
+            downs.append(near[at + pieces])
+            at += pieces + 1
     hidden = jnp.concatenate(hiddens, axis=1)
     common, common_downs = [], []
     for _ in range(shared):
@@ -363,23 +372,31 @@
         copy.wait()
 
 
-def join_kernel(key_ref, value_ref, out_ref, sems):
+def join_kernel(key_ref, value_ref, *refs):
+    count = (len(refs) - 2) // 2
+    rest, out_ref, copy_refs, sems = refs[:count], refs[count], refs[count + 1 : -1], refs[-1]
     width = key_ref.shape[1]
     run_copies(
-        [(key_ref, out_ref.at[:, :width]), (value_ref, out_ref.at[:, width:])], sems
-    )
-
-
-def split_kernel(gate_ref, up_ref, down_ref, *refs):
-    in_refs, out_refs, sems = refs[:2], refs[2:4], refs[4]
+        [(key_ref, out_ref.at[:, :width]), (value_ref, out_ref.at[:, width:])]
+        + list(zip(rest, copy_refs)),
+        sems,
+    )
+
+
+def split_kernel(
+    place_ref, routes_ref, weight_ref, gate_ref, up_ref, down_ref, marks_ref, *out_refs, cuts
+):
+    marks_ref[...] = route_marks(place_ref, routes_ref, weight_ref)
     half = gate_ref.shape[1] // 2
-    moves = []
-    for part in range(2):
+    at = 0
+    for part, pieces in enumerate(cuts):
         units = slice(part * half, (part + 1) * half)
-        moves.append((gate_ref.at[:, units], in_refs[part].at[:, :half]))
-        moves.append((up_ref.at[:, units], in_refs[part].at[:, half:]))
-        moves.append((down_ref.at[units, :], out_refs[part]))
-    run_copies(moves, sems)
+        for rows in pieces:
+            out_refs[at][:, :half] = gate_ref[rows, units]
+            out_refs[at][:, half:] = up_ref[rows, units]
+            at += 1
+        out_refs[at][...] = down_ref[units, :]
+        at += 1
 
 
 def gathered_body(
@@ -411,6 +428,9 @@
         ]
         return lax.ppermute(value, ("sp", "tp"), pairs)
 
+    def stay(value):
+        return pltpu.with_memory_space_constraint(value, pltpu.HBM)
+
     def near(value):
         return pltpu.with_memory_space_constraint(value, pltpu.VMEM)
 
@@ -428,40 +448,50 @@
     far = list(range(senders - 2, 0, -2))
     smem = pl.BlockSpec(memory_space=pltpu.SMEM)
 
-    own_routes = lax.dynamic_slice_in_dim(routes, column * rows_dev, rows_dev, 0)
-    marks = route_marks(own_routes, route_weight)
-
     anywhere = pl.BlockSpec(memory_space=pl.ANY)
-    kv_own = pl.pallas_call(
+    held = [query_maps, mix_lambda[None], head_gain[None]]
+    kv_own, query_maps, lambdas, gains = pl.pallas_call(
         join_kernel,
-        out_shape=pltpu.VMEM(
-            (key_maps.shape[0], key_maps.shape[1] + value_rows.shape[1]), key_maps.dtype
-        ),
-        in_specs=[anywhere] * 2,
-        out_specs=pl.BlockSpec(memory_space=pltpu.VMEM),
-        scratch_shapes=[pltpu.SemaphoreType.DMA((2,))],
+        out_shape=[
+            pltpu.VMEM(
+                (key_maps.shape[0], key_maps.shape[1] + value_rows.shape[1]), key_maps.dtype
+            )
+        ]
+        + [pltpu.VMEM(x.shape, x.dtype) for x in held],
+        in_specs=[anywhere] * 5,
+        out_specs=whole_vmem(4),
+        scratch_shapes=[pltpu.SemaphoreType.DMA((5,))],
         compiler_params=vmem_mib(4),
         name="join",
-    )(key_maps, value_rows)
+    )(*map(stay, [key_maps, value_rows] + held))
+    kv_side = swap(kv_own, 1, 0)
     kv_line = [swap(kv_own, mask, 0) for mask in far]
-    kv_side = [swap(block, 1, 0) for block in [kv_own] + kv_line]
-    kv_blocks = [kv_own] + kv_line + kv_side
-    query_maps, marks, place = lax.optimization_barrier((query_maps, marks, place))
-
+    kv_far = [swap(kv_side, mask, 0) for mask in far]
+    kv_blocks = [kv_own, kv_side] + kv_line + kv_far
     own_set = [expert_gate[0], expert_up[0], expert_down[0]]
     units = own_set[0].shape[1]
     half = units // 2
-    pack_a, pack_b, down_a, down_b = pl.pallas_call(
-        split_kernel,
-        out_shape=[pltpu.VMEM((width, units), own_set[0].dtype)] * 2
-        + [pltpu.VMEM((half, width), own_set[0].dtype)] * 2,
-        in_specs=[anywhere] * 3,
-        out_specs=whole_vmem(4),
-        scratch_shapes=[pltpu.SemaphoreType.DMA((6,))],
-        compiler_params=vmem_mib(4),
+    cut = 3 * width // 4
+    cuts = [[slice(0, width)], [slice(0, cut), slice(cut, width)]]
+    pack_shape = lambda rows: pltpu.VMEM((rows, units), own_set[0].dtype)
+    down_shape = pltpu.HBM((half, width), own_set[0].dtype)
+    marks, pack_a, down_a, pack_b, pack_c, down_b = pl.pallas_call(
+        partial(split_kernel, cuts=cuts),
+        out_shape=[
+            pltpu.VMEM((rows_dev, 128), jnp.bfloat16),
+            pack_shape(width),
+            down_shape,
+            pack_shape(cut),
+            pack_shape(width - cut),
+            down_shape,
+        ],
+        in_specs=[smem] + whole_vmem(5),
+        out_specs=whole_vmem(6),
+        compiler_params=vmem_mib(12),
         name="split",
-    )(*own_set)
+    )(place, *map(stay, [routes.T, route_weight.T] + own_set))
     b_in, a_in = swap(pack_b, 0, 2), swap(pack_a, 1, 0)
+    c_in = swap(pack_c, 0, 2)
     swapped = [swap(w, 0, 1) for w in own_set]
     shared_set = [shared_gate, shared_up, shared_down]
     shared_set = shared_set + [swap(w, 0, 1) for w in shared_set]
@@ -476,7 +506,7 @@
             score_scale=head_dim ** (-0.5),
         ),
         out_shape=[pltpu.VMEM((rows_dev, head_columns), jnp.bfloat16)] * columns,
-        in_specs=[smem, smem] + whole_vmem(2 + len(kv_blocks)),
+        in_specs=[smem] + whole_vmem(3 + len(kv_blocks)),
         out_specs=whole_vmem(columns),
         scratch_shapes=[
             pltpu.VMEM((kv_rows, kv_own.shape[1]), jnp.bfloat16),
@@ -485,7 +515,7 @@
         cost_estimate=kernel_cost(4e9),
         compiler_params=vmem_mib(20),
         name="attention",
-    )(place, mix_lambda, query_maps, head_gain[None], *map(near, kv_blocks))
+    )(place, *map(near, [lambdas, query_maps, gains] + kv_blocks))
     parts = [attended[0]] + [swap(attended[step], 0, step) for step in range(1, columns)]
     b_out, a_out = swap(down_b, 0, 2), swap(down_a, 1, 0)
 
@@ -508,10 +538,9 @@
 
     line = [packed] + [swap(packed, mask, 0) for mask in far]
     side = [swap(block, 1, 2) for block in line]
-    b_in, b_out = after((b_in, b_out), line[-1])
-    a_in, a_out = after((a_in, a_out), line[-1])
-    pack_set = [b_in, b_out, swap(b_in, 0, 1), swap(b_out, 0, 1)]
-    pack_set += [a_in, a_out, swap(a_in, 0, 1), swap(a_out, 0, 1)]
+    b_in, c_in, b_out, a_in, a_out = after((b_in, c_in, b_out, a_in, a_out), line[-1])
+    pack_set = [b_in, c_in, b_out] + [swap(w, 0, 1) for w in (b_in, c_in, b_out)]
+    pack_set += [a_in, a_out] + [swap(w, 0, 1) for w in (a_in, a_out)]
     own_set = own_set + swapped
 
     def experts(chosen, with_shared):
@@ -526,7 +555,7 @@
                 plain=2,
                 shared=2 if with_shared else 0,
                 packed_own=2,
-                packed_other=2,
+                packed_other=1,
             ),
             out_shape=[pltpu.VMEM((rows_dev, width), kind) for kind in kinds],
             in_specs=[smem] + whole_vmem(len(rows) + len(weights)),
@@ -539,18 +568,13 @@
     calls = [[0, 1], list(range(2, len(line)))] if len(line) > 2 else [list(range(len(line)))]
     masks = [0] + far
     total = stream.astype(jnp.float32)
-    ready = None
     for number, chosen in enumerate(calls):
-        if ready is not None:
-            for i in chosen:
-                line[i] = after(line[i], ready)
         outs = experts(chosen, number == 0)
         for spot in range(len(chosen) - 1, -1, -1):
             mask = masks[chosen[spot]]
             joined = outs[2 * spot] + swap(outs[2 * spot + 1], 1, 2).astype(jnp.float32)
             if mask:
                 joined = joined.astype(jnp.bfloat16)
-                ready = joined if ready is None else ready
                 joined = swap(joined, mask, 0).astype(jnp.float32)
             total = total + joined
     return total.astype(jnp.bfloat16)

time: 149 us -> 145 us (0.973)
  waiting for transfers between devices: 91.4 us -> 82.4 us
  starting transfers between devices: 38 us -> 44.7 us
  Pallas kernels: 12.8 us -> 16.7 us
  local copies, waits for them, and re-layouts: 3.94 us -> 0.05 us
    ppermute x38 -> x40, waiting for transfers between devices: 91.4 us -> 82.4 us  [swap(): return lax.ppermute(value, ('sp', 'tp'), pairs)]
    ppermute x38 -> x40, starting transfers between devices: 38 us -> 44.7 us  [swap(): return lax.ppermute(value, ('sp', 'tp'), pairs)]
    unnamed x30 -> x22, local copies, waits for them, and re-layouts: 3.86 us -> 0.05 us
    pallas_call x2, Pallas kernels: 0.54 us -> 4.33 us  [the longest x1 3.33 us: gathered_body(): pl.pallas_call(partial(split_kernel, cuts=cuts), out_shape=[pltpu.VMEM((r...]
  transfers between devices with their start and end apart: 38 -> 40, of which waited for: 22 -> 18; matrix products, arithmetic and copies ran while one was open for 1% -> 0% of each run, Pallas kernels for 3% -> 9%
where the time goes in v1:
time: 145 us
  waiting for transfers between devices  82.4 us (57%)
  starting transfers between devices  44.7 us (31%)
  Pallas kernels  16.7 us (12%)
    ppermute x40, waiting for transfers between devices, swap(): return lax.ppermute(value, ('sp', 'tp'), pairs)  82.4 us
    ppermute x40, starting transfers between devices, swap(): return lax.ppermute(value, ('sp', 'tp'), pairs)  44.7 us
    pallas_call x2, Pallas kernels, experts(): pl.pallas_call(partial(expert_kernel, pairs=len(chosen), weights=len(weig...  7.52 us
    pallas_call x1, Pallas kernels, gathered_body(): pl.pallas_call(partial(split_kernel, cuts=cuts), out_shape=[pltpu.VMEM((r...  3.33 us
    pallas_call x1, Pallas kernels, gathered_body(): pl.pallas_call(partial(attention_kernel, blocks=len(kv_blocks), kv_local=...  2.92 us
  transfers between devices with their start and end apart: 40, of which 18 were waited for; matrix products, arithmetic and copies ran while one was open for 0% of the time, Pallas kernels for 9%

profile of v1, /device:TPU:0, one launch (start us, length us, event | category | flops | bytes accessed | tf_op | source)
XLA Modules:
  0.0 145.1 jit_solution(5723861099001887647)
XLA Ops:
  0.0 1.0 join.1
  1.0 3.0 %collective-permute-start = (bf16[192,256]{1,0:T(8,128)(2,1)S(1)}, bf16[192,256]{1,0:T(8,128)(2,1)S(1)}, u32[]{:S(2)}, u32[]{:S(2)}) collective-permute-start(bf16[192,256]{1,0:T(8,128)(2,1)S(1)} %get-tuple-element.38.refs_0_), channel_id=1, source_target_pairs={{0,4},{1,5},{2,6},{3,7},{4,0},{5,1},{6,2},{7,3},{8,12},{9,13},{10,... | collective-permute-start | bytes 294920 | tf_op jit(solution)/shard_map/ppermute | solution.py:429
  4.0 3.6 %collective-permute-start.1 = (bf16[192,256]{1,0:T(8,128)(2,1)S(1)}, bf16[192,256]{1,0:T(8,128)(2,1)S(1)}, u32[]{:S(2)}, u32[]{:S(2)}) collective-permute-start(bf16[192,256]{1,0:T(8,128)(2,1)S(1)} %get-tuple-element.38.refs_0_), channel_id=1, source_target_pairs={{0,24},{1,25},{2,26},{3,27},{4,28},{5,29},{6,30},{7,31},{8,16},{9,... | collective-permute-start | bytes 294920 | tf_op jit(solution)/shard_map/ppermute | solution.py:429
  7.6 0.8 collective-permute-start.3
  8.4 3.6 %collective-permute-start.4 = (bf16[192,256]{1,0:T(8,128)(2,1)S(1)}, bf16[192,256]{1,0:T(8,128)(2,1)S(1)}, u32[]{:S(2)}, u32[]{:S(2)}) collective-permute-start(bf16[192,256]{1,0:T(8,128)(2,1)S(1)} %collective-permute-done.refs_1_), channel_id=1, source_target_pairs={{0,24},{1,25},{2,26},{3,27},{4,28},{5,29},{6,30},{7,31},{8,16},{9,... | collective-permute-start | bytes 294920 | tf_op jit(solution)/shard_map/ppermute | solution.py:429
  12.0 3.8 %collective-permute-start.6 = (bf16[192,256]{1,0:T(8,128)(2,1)S(1)}, bf16[192,256]{1,0:T(8,128)(2,1)S(1)}, u32[]{:S(2)}, u32[]{:S(2)}) collective-permute-start(bf16[192,256]{1,0:T(8,128)(2,1)S(1)} %collective-permute-done.refs_1_), channel_id=1, source_target_pairs={{0,8},{1,9},{2,10},{3,11},{4,12},{5,13},{6,14},{7,15},{8,0},{9,1},... | collective-permute-start | bytes 294920 | tf_op jit(solution)/shard_map/ppermute | solution.py:429
  15.9 4.9 %collective-permute-done.2.refs_3_ = bf16[192,256]{1,0:T(8,128)(2,1)S(1)} collective-permute-done((bf16[192,256]{1,0:T(8,128)(2,1)S(1)}, bf16[192,256]{1,0:T(8,128)(2,1)S(1)}, u32[]{:S(2)}, u32[]{:S(2)}) %collective-permute-start.2) | collective-permute-done | bytes 98336 | tf_op jit(solution)/shard_map/ppermute | solution.py:429
  20.8 3.3 %collective-permute-done.5.refs_6_ = bf16[192,256]{1,0:T(8,128)(2,1)S(1)} collective-permute-done((bf16[192,256]{1,0:T(8,128)(2,1)S(1)}, bf16[192,256]{1,0:T(8,128)(2,1)S(1)}, u32[]{:S(2)}, u32[]{:S(2)}) %collective-permute-start.5) | collective-permute-done | bytes 98336 | tf_op jit(solution)/shard_map/ppermute | solution.py:429
  24.1 2.9 %attention.1 = (bf16[48,256]{1,0:T(8,128)(2,1)S(1)}, bf16[48,256]{1,0:T(8,128)(2,1)S(1)}, bf16[48,256]{1,0:T(8,128)(2,1)S(1)}, bf16[48,256]{1,0:T(8,128)(2,1)S(1)}) custom-call(s32[3]{0:T(128)S(1)} %pad_add_fusion.place_ref, f32[1,2]{1,0:T(1,128)S(1)} %get-tuple-element.35.lambda_ref, bf16[192,256]{1,0:T(8,128)(2,1)S(1)} %get-tuple-element.36.query_ref, ...), custom_call_target="tpu_custom_call" | custom-call | flops 4000000000 | tf_op jit(solution)/shard_map/attention/pallas_call | solution.py:501
  27.1 1.6 %collective-permute-start.8 = (bf16[48,256]{1,0:T(8,128)(2,1)S(1)}, bf16[48,256]{1,0:T(8,128)(2,1)S(1)}, u32[]{:S(2)}, u32[]{:S(2)}) collective-permute-start(bf16[48,256]{1,0:T(8,128)(2,1)S(1)} %get-tuple-element.41), channel_id=1, source_target_pairs={{0,2},{1,3},{2,0},{3,1},{4,6},{5,7},{6,4},{7,5},{8,10},{9,11},{10,... | collective-permute-start | bytes 73736 | tf_op jit(solution)/shard_map/ppermute | solution.py:429
  28.9 3.3 %split.1 = (bf16[48,128]{1,0:T(8,128)(2,1)S(1)}, bf16[2048,256]{1,0:T(8,128)(2,1)S(1)}, bf16[128,2048]{1,0:T(8,128)(2,1)}, bf16[1536,256]{1,0:T(8,128)(2,1)S(1)}...) custom-call(s32[3]{0:T(128)S(1)} %pad_add_fusion.place_ref, s32[4,192]{1,0:T(4,128)} %bitcast.24, ...), custom_call_target="tpu_custom_call" | custom-call | tf_op jit(solution)/shard_map/split/pallas_call | solution.py:478
  32.3 1.6 %collective-permute-start.17 = (bf16[512,256]{1,0:T(8,128)(2,1)S(1)}, bf16[512,256]{1,0:T(8,128)(2,1)S(1)}, u32[]{:S(2)}, u32[]{:S(2)}) collective-permute-start(bf16[512,256]{1,0:T(8,128)(2,1)S(1)} %get-tuple-element.46), channel_id=1, source_target_pairs={{0,2},{1,3},{2,0},{3,1},{4,6},{5,7},{6,4},{7,5},{8,10},{9,11},{10,... | collective-permute-start | bytes 786440 | tf_op jit(solution)/shard_map/ppermute | solution.py:429
  34.0 1.9 %project.1 = (bf16[48,2048]{1,0:T(8,128)(2,1)S(1)}, bf16[48,2176]{1,0:T(8,128)(2,1)S(1)}) custom-call(s32[3]{0:T(128)S(1)} %pad_add_fusion.place_ref, bf16[1024,2048]{1,0:T(8,128)(2,1)S(1)} %copy-done.3, bf16[48,2048]{1,0:T(8,128)(2,1)S(1)} %copy-done.7, f32[1,2048]{1,0:T(1,128)S(1)} %bitcast.23, bf16[48,128]{1,0:T(8,128)(2,1)S(1)} %get-tuple-element.34.marks_ref, ...), custom_call_target="tpu_custom_call" | custom-call | flops 2000000000 | tf_op jit(solution)/shard_map/project/pallas_call | solution.py:522
  35.9 2.5 %collective-permute-start.11 = (bf16[48,2176]{1,0:T(8,128)(2,1)S(1)}, bf16[48,2176]{1,0:T(8,128)(2,1)S(1)}, u32[]{:S(2)}, u32[]{:S(2)}) collective-permute-start(bf16[48,2176]{1,0:T(8,128)(2,1)S(1)} %get-tuple-element.44.refs_0_), channel_id=1, source_target_pairs={{0,24},{1,25},{2,26},{3,27},{4,28},{5,29},{6,30},{7,31},{8,16},{9,... | collective-permute-start | bytes 626696 | tf_op jit(solution)/shard_map/ppermute | solution.py:429
  38.5 0.5 collective-permute-start.19
  39.0 0.5 collective-permute-start.18
  39.5 1.4 collective-permute-done.17.refs_11_
  41.0 1.5 %collective-permute-start.10 = (bf16[48,2176]{1,0:T(8,128)(2,1)S(1)}, bf16[48,2176]{1,0:T(8,128)(2,1)S(1)}, u32[]{:S(2)}, u32[]{:S(2)}) collective-permute-start(bf16[48,2176]{1,0:T(8,128)(2,1)S(1)} %get-tuple-element.44.refs_0_), channel_id=1, source_target_pairs={{0,6},{1,7},{2,4},{3,5},{4,2},{5,3},{6,0},{7,1},{8,14},{9,15},{10,... | collective-permute-start | bytes 626696 | tf_op jit(solution)/shard_map/ppermute | solution.py:429
  42.5 0.6 collective-permute-done.21.refs_2_
  43.1 4.6 %collective-permute-start.33 = (bf16[48,2176]{1,0:T(8,128)(2,1)S(1)}, bf16[48,2176]{1,0:T(8,128)(2,1)S(1)}, u32[]{:S(2)}, u32[]{:S(2)}) collective-permute-start(bf16[48,2176]{1,0:T(8,128)(2,1)S(1)} %get-tuple-element.44.refs_0_), channel_id=1, source_target_pairs={{0,16},{1,17},{2,18},{3,19},{4,20},{5,21},{6,22},{7,23},{8,24},{9,... | collective-permute-start | bytes 626696 | tf_op jit(solution)/shard_map/ppermute | solution.py:429
  47.6 1.4 collective-permute-done.11.refs_2_
  49.0 0.5 collective-permute-start.20
  49.5 19.4 %collective-permute-done.10.refs_1_ = bf16[48,2176]{1,0:T(8,128)(2,1)S(1)} collective-permute-done((bf16[48,2176]{1,0:T(8,128)(2,1)S(1)}, bf16[48,2176]{1,0:T(8,128)(2,1)S(1)}, u32[]{:S(2)}, u32[]{:S(2)}) %collective-permute-start.10) | collective-permute-done | bytes 208928 | tf_op jit(solution)/shard_map/ppermute | solution.py:429
  68.9 1.6 %collective-permute-start.16 = (bf16[1536,256]{1,0:T(8,128)(2,1)S(1)}, bf16[1536,256]{1,0:T(8,128)(2,1)S(1)}, u32[]{:S(2)}, u32[]{:S(2)}) collective-permute-start(bf16[1536,256]{1,0:T(8,128)(2,1)S(1)} %get-tuple-element.45), channel_id=1, source_target_pairs={{0,2},{1,3},{2,0},{3,1},{4,6},{5,7},{6,4},{7,5},{8,10},{9,11},{10,... | collective-permute-start | bytes 2359304 | tf_op jit(solution)/shard_map/ppermute | solution.py:429
  70.7 8.4 %collective-permute-done.20.refs_17_ = bf16[128,2048]{1,0:T(8,128)(2,1)S(1)} collective-permute-done((bf16[128,2048]{1,0:T(8,128)(2,1)S(1)}, bf16[128,2048]{1,0:T(8,128)(2,1)S(1)}, u32[]{:S(2)}, u32[]{:S(2)}) %collective-permute-start.20) | collective-permute-done | bytes 524320 | tf_op jit(solution)/shard_map/ppermute | solution.py:429
  79.5 6.5 %collective-permute-done.12.refs_3_ = bf16[48,2176]{1,0:T(8,128)(2,1)S(1)} collective-permute-done((bf16[48,2176]{1,0:T(8,128)(2,1)S(1)}, bf16[48,2176]{1,0:T(8,128)(2,1)S(1)}, u32[]{:S(2)}, u32[]{:S(2)}) %collective-permute-start.12) | collective-permute-done | bytes 208928 | tf_op jit(solution)/shard_map/ppermute | solution.py:429
  86.1 7.3 %collective-permute-done.16.refs_10_ = bf16[1536,256]{1,0:T(8,128)(2,1)S(1)} collective-permute-done((bf16[1536,256]{1,0:T(8,128)(2,1)S(1)}, bf16[1536,256]{1,0:T(8,128)(2,1)S(1)}, u32[]{:S(2)}, u32[]{:S(2)}) %collective-permute-start.16) | collective-permute-done | bytes 786464 | tf_op jit(solution)/shard_map/ppermute | solution.py:429
  94.5 1.5 %collective-permute-done.27.refs_23_ = bf16[2048,256]{1,0:T(8,128)(2,1)S(1)} collective-permute-done((bf16[2048,256]{1,0:T(8,128)(2,1)S(1)}, bf16[2048,256]{1,0:T(8,128)(2,1)S(1)}, u32[]{:S(2)}, u32[]{:S(2)}) %collective-permute-start.27) | collective-permute-done | bytes 1048608 | tf_op jit(solution)/shard_map/ppermute | solution.py:429
  96.2 1.4 collective-permute-done.28.refs_24_
  97.7 1.4 collective-permute-done.29.refs_25_
  99.2 4.4 %collective-permute-done.23.refs_14_ = bf16[512,256]{1,0:T(8,128)(2,1)S(1)} collective-permute-done((bf16[512,256]{1,0:T(8,128)(2,1)S(1)}, bf16[512,256]{1,0:T(8,128)(2,1)S(1)}, u32[]{:S(2)}, u32[]{:S(2)}) %collective-permute-start.23) | collective-permute-done | bytes 262176 | tf_op jit(solution)/shard_map/ppermute | solution.py:429
  103.5 1.5 %collective-permute-start.35 = (bf16[48,2176]{1,0:T(8,128)(2,1)S(1)}, bf16[48,2176]{1,0:T(8,128)(2,1)S(1)}, u32[]{:S(2)}, u32[]{:S(2)}) collective-permute-start(bf16[48,2176]{1,0:T(8,128)(2,1)S(1)} %collective-permute-done.21.refs_2_), channel_id=1, source_target_pairs={{0,6},{1,7},{2,4},{3,5},{4,2},{5,3},{6,0},{7,1},{8,14},{9,15},{10,... | collective-permute-start | bytes 626696 | tf_op jit(solution)/shard_map/ppermute | solution.py:429
  105.0 1.4 collective-permute-start.34
  106.5 4.3 %experts.2 = (f32[48,2048]{1,0:T(8,128)S(1)}, bf16[48,2048]{1,0:T(8,128)(2,1)S(1)}, f32[48,2048]{1,0:T(8,128)S(1)}, bf16[48,2048]{1,0:T(8,128)(2,1)S(1)}) custom-call(s32[3]{0:T(128)S(1)} %pad_add_fusion.place_ref, bf16[48,2176]{1,0:T(8,128)(2,1)S(1)} %get-tuple-element.44.refs_0_, bf16[48,2176]{1,0:T(8,128)(2,1)S(1)} %collective-permute-done.10.refs_1_, ...), custom_call_target="tpu_custom_call" | custom-call | flops 6000000000 | tf_op jit(solution)/shard_map/experts/pallas_call | solution.py:550
  110.8 1.6 %collective-permute-start.30 = (bf16[48,2048]{1,0:T(8,128)(2,1)S(1)}, bf16[48,2048]{1,0:T(8,128)(2,1)S(1)}, u32[]{:S(2)}, u32[]{:S(2)}) collective-permute-start(bf16[48,2048]{1,0:T(8,128)(2,1)S(1)} %get-tuple-element.56), channel_id=1, source_target_pairs={{0,6},{1,7},{2,4},{3,5},{4,2},{5,3},{6,0},{7,1},{8,14},{9,15},{10,... | collective-permute-start | bytes 589832 | tf_op jit(solution)/shard_map/ppermute | solution.py:429
  112.3 1.4 collective-permute-start.32
  113.8 3.2 %collective-permute-done.34.refs_1_ = bf16[48,2176]{1,0:T(8,128)(2,1)S(1)} collective-permute-done((bf16[48,2176]{1,0:T(8,128)(2,1)S(1)}, bf16[48,2176]{1,0:T(8,128)(2,1)S(1)}, u32[]{:S(2)}, u32[]{:S(2)}) %collective-permute-start.34) | collective-permute-done | bytes 208928 | tf_op jit(solution)/shard_map/ppermute | solution.py:429
  117.0 3.2 %experts.3 = (f32[48,2048]{1,0:T(8,128)S(1)}, bf16[48,2048]{1,0:T(8,128)(2,1)S(1)}, f32[48,2048]{1,0:T(8,128)S(1)}, bf16[48,2048]{1,0:T(8,128)(2,1)S(1)}) custom-call(s32[3]{0:T(128)S(1)} %pad_add_fusion.place_ref, bf16[48,2176]{1,0:T(8,128)(2,1)S(1)} %collective-permute-done.33.refs_0_, bf16[48,2176]{1,0:T(8,128)(2,1)S(1)} %collective-permute-done.34.refs_1_, ...), custom_call_target="tpu_custom_call" | custom-call | flops 6000000000 | tf_op jit(solution)/shard_map/experts/pallas_call | solution.py:550
  120.2 1.6 %collective-permute-start.36 = (bf16[48,2048]{1,0:T(8,128)(2,1)S(1)}, bf16[48,2048]{1,0:T(8,128)(2,1)S(1)}, u32[]{:S(2)}, u32[]{:S(2)}) collective-permute-start(bf16[48,2048]{1,0:T(8,128)(2,1)S(1)} %get-tuple-element.60), channel_id=1, source_target_pairs={{0,6},{1,7},{2,4},{3,5},{4,2},{5,3},{6,0},{7,1},{8,14},{9,15},{10,... | collective-permute-start | bytes 589832 | tf_op jit(solution)/shard_map/ppermute | solution.py:429
  121.7 1.4 collective-permute-start.38
  123.2 1.4 collective-permute-start.31
  124.6 5.0 %collective-permute-done.36 = bf16[48,2048]{1,0:T(8,128)(2,1)S(1)} collective-permute-done((bf16[48,2048]{1,0:T(8,128)(2,1)S(1)}, bf16[48,2048]{1,0:T(8,128)(2,1)S(1)}, u32[]{:S(2)}, u32[]{:S(2)}) %collective-permute-start.36) | collective-permute-done | bytes 196640 | tf_op jit(solution)/shard_map/ppermute | solution.py:429
  129.6 1.1 collective-permute-start.37
  130.7 2.2 %collective-permute-done.38 = bf16[48,2048]{1,0:T(8,128)(2,1)S(1)} collective-permute-done((bf16[48,2048]{1,0:T(8,128)(2,1)S(1)}, bf16[48,2048]{1,0:T(8,128)(2,1)S(1)}, u32[]{:S(2)}, u32[]{:S(2)}) %collective-permute-start.38) | collective-permute-done | bytes 196640 | tf_op jit(solution)/shard_map/ppermute | solution.py:429
  133.0 1.0 collective-permute-start.39
  134.0 1.3 collective-permute-done.37
  135.4 8.9 %collective-permute-done.39 = bf16[48,2048]{1,0:T(8,128)(2,1)S(1)} collective-permute-done((bf16[48,2048]{1,0:T(8,128)(2,1)S(1)}, bf16[48,2048]{1,0:T(8,128)(2,1)S(1)}, u32[]{:S(2)}, u32[]{:S(2)}) %collective-permute-start.39) | collective-permute-done | bytes 196640 | tf_op jit(solution)/shard_map/ppermute | solution.py:429
  144.3 0.8 add_convert_fusion
  (65 shorter events, 2.9 us)
Async XLA Ops:
  1.0 7.4 %collective-permute-start = (bf16[192,256]{1,0:T(8,128)(2,1)S(1)}, bf16[192,256]{1,0:T(8,128)(2,1)S(1)}, u32[]{:S(2)}, u32[]{:S(2)}) collective-permute-start(bf16[192,256]{1,0:T(8,128)(2,1)S(1)} %get-tuple-element.38.refs_0_), channel_id=1, source_target_pairs={{0,4},{1,5},{2,6},{3,7},{4,0},{5,1},{6,2},{7,3},{8,12},{9,13},{10,... | collective-permute-start | bytes 294920 | tf_op jit(solution)/shard_map/ppermute | solution.py:429
  4.0 8.0 %collective-permute-start.1 = (bf16[192,256]{1,0:T(8,128)(2,1)S(1)}, bf16[192,256]{1,0:T(8,128)(2,1)S(1)}, u32[]{:S(2)}, u32[]{:S(2)}) collective-permute-start(bf16[192,256]{1,0:T(8,128)(2,1)S(1)} %get-tuple-element.38.refs_0_), channel_id=1, source_target_pairs={{0,24},{1,25},{2,26},{3,27},{4,28},{5,29},{6,30},{7,31},{8,16},{9,... | collective-permute-start | bytes 294920 | tf_op jit(solution)/shard_map/ppermute | solution.py:429
  7.6 13.1 %collective-permute-start.2 = (bf16[192,256]{1,0:T(8,128)(2,1)S(1)}, bf16[192,256]{1,0:T(8,128)(2,1)S(1)}, u32[]{:S(2)}, u32[]{:S(2)}) collective-permute-start(bf16[192,256]{1,0:T(8,128)(2,1)S(1)} %get-tuple-element.38.refs_0_), channel_id=1, source_target_pairs={{0,16},{1,17},{2,18},{3,19},{4,20},{5,21},{6,22},{7,23},{8,24},{9,... | collective-permute-start | bytes 294920 | tf_op jit(solution)/shard_map/ppermute | solution.py:429
  7.6 13.1 %collective-permute-start.3 = (bf16[192,256]{1,0:T(8,128)(2,1)S(1)}, bf16[192,256]{1,0:T(8,128)(2,1)S(1)}, u32[]{:S(2)}, u32[]{:S(2)}) collective-permute-start(bf16[192,256]{1,0:T(8,128)(2,1)S(1)} %get-tuple-element.38.refs_0_), channel_id=1, source_target_pairs={{0,8},{1,9},{2,10},{3,11},{4,12},{5,13},{6,14},{7,15},{8,0},{9,1},... | collective-permute-start | bytes 294920 | tf_op jit(solution)/shard_map/ppermute | solution.py:429
  8.4 12.4 %collective-permute-start.4 = (bf16[192,256]{1,0:T(8,128)(2,1)S(1)}, bf16[192,256]{1,0:T(8,128)(2,1)S(1)}, u32[]{:S(2)}, u32[]{:S(2)}) collective-permute-start(bf16[192,256]{1,0:T(8,128)(2,1)S(1)} %collective-permute-done.refs_1_), channel_id=1, source_target_pairs={{0,24},{1,25},{2,26},{3,27},{4,28},{5,29},{6,30},{7,31},{8,16},{9,... | collective-permute-start | bytes 294920 | tf_op jit(solution)/shard_map/ppermute | solution.py:429
  12.0 12.0 %collective-permute-start.5 = (bf16[192,256]{1,0:T(8,128)(2,1)S(1)}, bf16[192,256]{1,0:T(8,128)(2,1)S(1)}, u32[]{:S(2)}, u32[]{:S(2)}) collective-permute-start(bf16[192,256]{1,0:T(8,128)(2,1)S(1)} %collective-permute-done.refs_1_), channel_id=1, source_target_pairs={{0,16},{1,17},{2,18},{3,19},{4,20},{5,21},{6,22},{7,23},{8,24},{9,... | collective-permute-start | bytes 294920 | tf_op jit(solution)/shard_map/ppermute | solution.py:429
  12.0 12.0 %collective-permute-start.6 = (bf16[192,256]{1,0:T(8,128)(2,1)S(1)}, bf16[192,256]{1,0:T(8,128)(2,1)S(1)}, u32[]{:S(2)}, u32[]{:S(2)}) collective-permute-start(bf16[192,256]{1,0:T(8,128)(2,1)S(1)} %collective-permute-done.refs_1_), channel_id=1, source_target_pairs={{0,8},{1,9},{2,10},{3,11},{4,12},{5,13},{6,14},{7,15},{8,0},{9,1},... | collective-permute-start | bytes 294920 | tf_op jit(solution)/shard_map/ppermute | solution.py:429
  24.1 9.9 %copy-start.8 = (f32[2048]{0:T(1024)S(1)}, f32[2048]{0:T(1024)}, u32[]{:S(2)}) copy-start(f32[2048]{0:T(1024)} %param.23) | copy-start | bytes 24580
  27.0 6.9 %collective-permute-start.7 = (bf16[48,256]{1,0:T(8,128)(2,1)S(1)}, bf16[48,256]{1,0:T(8,128)(2,1)S(1)}, u32[]{:S(2)}, u32[]{:S(2)}) collective-permute-start(bf16[48,256]{1,0:T(8,128)(2,1)S(1)} %get-tuple-element.40), channel_id=1, source_target_pairs={{0,1},{1,0},{2,3},{3,2},{4,5},{5,4},{6,7},{7,6},{8,9},{9,8},{10,11... | collective-permute-start | bytes 73736 | tf_op jit(solution)/shard_map/ppermute | solution.py:429
  27.1 6.8 %collective-permute-start.8 = (bf16[48,256]{1,0:T(8,128)(2,1)S(1)}, bf16[48,256]{1,0:T(8,128)(2,1)S(1)}, u32[]{:S(2)}, u32[]{:S(2)}) collective-permute-start(bf16[48,256]{1,0:T(8,128)(2,1)S(1)} %get-tuple-element.41), channel_id=1, source_target_pairs={{0,2},{1,3},{2,0},{3,1},{4,6},{5,7},{6,4},{7,5},{8,10},{9,11},{10,... | collective-permute-start | bytes 73736 | tf_op jit(solution)/shard_map/ppermute | solution.py:429
  28.7 5.3 %collective-permute-start.9 = (bf16[48,256]{1,0:T(8,128)(2,1)S(1)}, bf16[48,256]{1,0:T(8,128)(2,1)S(1)}, u32[]{:S(2)}, u32[]{:S(2)}) collective-permute-start(bf16[48,256]{1,0:T(8,128)(2,1)S(1)} %get-tuple-element.42), channel_id=1, source_target_pairs={{0,3},{1,2},{2,1},{3,0},{4,7},{5,6},{6,5},{7,4},{8,11},{9,10},{10,... | collective-permute-start | bytes 73736 | tf_op jit(solution)/shard_map/ppermute | solution.py:429
  32.3 16.7 %copy-start.9 = (bf16[128,2048]{1,0:T(8,128)(2,1)S(1)}, bf16[128,2048]{1,0:T(8,128)(2,1)}, u32[]{:S(2)}) copy-start(bf16[128,2048]{1,0:T(8,128)(2,1)} %get-tuple-element.49) | copy-start | bytes 1572868
  32.3 36.7 %copy-start = (bf16[1,2048,256]{2,1,0:T(8,128)(2,1)S(1)}, bf16[1,2048,256]{2,1,0:T(8,128)(2,1)}, u32[]{:S(2)}) copy-start(bf16[1,2048,256]{2,1,0:T(8,128)(2,1)} %param.26) | copy-start | bytes 3145732
  32.3 38.3 %copy-start.1 = (bf16[1,2048,256]{2,1,0:T(8,128)(2,1)S(1)}, bf16[1,2048,256]{2,1,0:T(8,128)(2,1)}, u32[]{:S(2)}) copy-start(bf16[1,2048,256]{2,1,0:T(8,128)(2,1)} %param.27) | copy-start | bytes 3145732
  32.3 53.8 %copy-start.2 = (bf16[1,256,2048]{2,1,0:T(8,128)(2,1)S(1)}, bf16[1,256,2048]{2,1,0:T(8,128)(2,1)}, u32[]{:S(2)}) copy-start(bf16[1,256,2048]{2,1,0:T(8,128)(2,1)} %param.28) | copy-start | bytes 3145732
  32.3 61.1 %copy-start.4 = (bf16[2048,256]{1,0:T(8,128)(2,1)S(1)}, bf16[2048,256]{1,0:T(8,128)(2,1)}, u32[]{:S(2)}) copy-start(bf16[2048,256]{1,0:T(8,128)(2,1)} %refs_20_.1) | copy-start | bytes 3145732
  32.3 61.1 %copy-start.5 = (bf16[2048,256]{1,0:T(8,128)(2,1)S(1)}, bf16[2048,256]{1,0:T(8,128)(2,1)}, u32[]{:S(2)}) copy-start(bf16[2048,256]{1,0:T(8,128)(2,1)} %refs_21_.1) | copy-start | bytes 3145732
  32.3 61.6 %copy-start.6 = (bf16[256,2048]{1,0:T(8,128)(2,1)S(1)}, bf16[256,2048]{1,0:T(8,128)(2,1)}, u32[]{:S(2)}) copy-start(bf16[256,2048]{1,0:T(8,128)(2,1)} %refs_22_.1) | copy-start | bytes 3145732
  32.3 8.6 %collective-permute-start.17 = (bf16[512,256]{1,0:T(8,128)(2,1)S(1)}, bf16[512,256]{1,0:T(8,128)(2,1)S(1)}, u32[]{:S(2)}, u32[]{:S(2)}) collective-permute-start(bf16[512,256]{1,0:T(8,128)(2,1)S(1)} %get-tuple-element.46), channel_id=1, source_target_pairs={{0,2},{1,3},{2,0},{3,1},{4,6},{5,7},{6,4},{7,5},{8,10},{9,11},{10,... | collective-permute-start | bytes 786440 | tf_op jit(solution)/shard_map/ppermute | solution.py:429
  35.9 7.2 %collective-permute-start.21 = (bf16[48,2176]{1,0:T(8,128)(2,1)S(1)}, bf16[48,2176]{1,0:T(8,128)(2,1)S(1)}, u32[]{:S(2)}, u32[]{:S(2)}) collective-permute-start(bf16[48,2176]{1,0:T(8,128)(2,1)S(1)} %get-tuple-element.44.refs_0_), channel_id=1, source_target_pairs={{0,8},{1,9},{2,10},{3,11},{4,12},{5,13},{6,14},{7,15},{8,0},{9,1},... | collective-permute-start | bytes 626696 | tf_op jit(solution)/shard_map/ppermute | solution.py:429
  35.9 13.1 %collective-permute-start.11 = (bf16[48,2176]{1,0:T(8,128)(2,1)S(1)}, bf16[48,2176]{1,0:T(8,128)(2,1)S(1)}, u32[]{:S(2)}, u32[]{:S(2)}) collective-permute-start(bf16[48,2176]{1,0:T(8,128)(2,1)S(1)} %get-tuple-element.44.refs_0_), channel_id=1, source_target_pairs={{0,24},{1,25},{2,26},{3,27},{4,28},{5,29},{6,30},{7,31},{8,16},{9,... | collective-permute-start | bytes 626696 | tf_op jit(solution)/shard_map/ppermute | solution.py:429
  38.5 54.9 %collective-permute-start.19 = (bf16[2048,256]{1,0:T(8,128)(2,1)S(1)}, bf16[2048,256]{1,0:T(8,128)(2,1)S(1)}, u32[]{:S(2)}, u32[]{:S(2)}) collective-permute-start(bf16[2048,256]{1,0:T(8,128)(2,1)S(1)} %get-tuple-element.48), channel_id=1, source_target_pairs={{0,4},{1,5},{2,6},{3,7},{4,0},{5,1},{6,2},{7,3},{8,12},{9,13},{10,... | collective-permute-start | bytes 3145736 | tf_op jit(solution)/shard_map/ppermute | solution.py:429
  39.0 31.5 %collective-permute-start.18 = (bf16[128,2048]{1,0:T(8,128)(2,1)S(1)}, bf16[128,2048]{1,0:T(8,128)(2,1)S(1)}, u32[]{:S(2)}, u32[]{:S(2)}) collective-permute-start(bf16[128,2048]{1,0:T(8,128)(2,1)S(1)} %copy-done.10), channel_id=1, source_target_pairs={{0,2},{1,3},{2,0},{3,1},{4,6},{5,7},{6,4},{7,5},{8,10},{9,11},{10,... | collective-permute-start | bytes 1572872 | tf_op jit(solution)/shard_map/ppermute | solution.py:429
  41.0 28.0 %collective-permute-start.10 = (bf16[48,2176]{1,0:T(8,128)(2,1)S(1)}, bf16[48,2176]{1,0:T(8,128)(2,1)S(1)}, u32[]{:S(2)}, u32[]{:S(2)}) collective-permute-start(bf16[48,2176]{1,0:T(8,128)(2,1)S(1)} %get-tuple-element.44.refs_0_), channel_id=1, source_target_pairs={{0,6},{1,7},{2,4},{3,5},{4,2},{5,3},{6,0},{7,1},{8,14},{9,15},{10,... | collective-permute-start | bytes 626696 | tf_op jit(solution)/shard_map/ppermute | solution.py:429
  43.1 25.9 %collective-permute-start.33 = (bf16[48,2176]{1,0:T(8,128)(2,1)S(1)}, bf16[48,2176]{1,0:T(8,128)(2,1)S(1)}, u32[]{:S(2)}, u32[]{:S(2)}) collective-permute-start(bf16[48,2176]{1,0:T(8,128)(2,1)S(1)} %get-tuple-element.44.refs_0_), channel_id=1, source_target_pairs={{0,16},{1,17},{2,18},{3,19},{4,20},{5,21},{6,22},{7,23},{8,24},{9,... | collective-permute-start | bytes 626696 | tf_op jit(solution)/shard_map/ppermute | solution.py:429
  49.0 30.1 %collective-permute-start.20 = (bf16[128,2048]{1,0:T(8,128)(2,1)S(1)}, bf16[128,2048]{1,0:T(8,128)(2,1)S(1)}, u32[]{:S(2)}, u32[]{:S(2)}) collective-permute-start(bf16[128,2048]{1,0:T(8,128)(2,1)S(1)} %copy-done.9), channel_id=1, source_target_pairs={{0,4},{1,5},{2,6},{3,7},{4,0},{5,1},{6,2},{7,3},{8,12},{9,13},{10,... | collective-permute-start | bytes 1572872 | tf_op jit(solution)/shard_map/ppermute | solution.py:429
  68.9 25.0 %collective-permute-start.13 = (bf16[2048,256]{1,0:T(8,128)(2,1)S(1)}, bf16[2048,256]{1,0:T(8,128)(2,1)S(1)}, u32[]{:S(2)}, u32[]{:S(2)}) collective-permute-start(bf16[2048,256]{1,0:T(8,128)(2,1)S(1)} %bitcast.12), channel_id=1, source_target_pairs={{0,1},{1,0},{2,3},{3,2},{4,5},{5,4},{6,7},{7,6},{8,9},{9,8},{10,11... | collective-permute-start | bytes 3145736 | tf_op jit(solution)/shard_map/ppermute | solution.py:429
  68.9 24.4 %collective-permute-start.16 = (bf16[1536,256]{1,0:T(8,128)(2,1)S(1)}, bf16[1536,256]{1,0:T(8,128)(2,1)S(1)}, u32[]{:S(2)}, u32[]{:S(2)}) collective-permute-start(bf16[1536,256]{1,0:T(8,128)(2,1)S(1)} %get-tuple-element.45), channel_id=1, source_target_pairs={{0,2},{1,3},{2,0},{3,1},{4,6},{5,7},{6,4},{7,5},{8,10},{9,11},{10,... | collective-permute-start | bytes 2359304 | tf_op jit(solution)/shard_map/ppermute | solution.py:429
  70.5 23.5 %collective-permute-start.14 = (bf16[2048,256]{1,0:T(8,128)(2,1)S(1)}, bf16[2048,256]{1,0:T(8,128)(2,1)S(1)}, u32[]{:S(2)}, u32[]{:S(2)}) collective-permute-start(bf16[2048,256]{1,0:T(8,128)(2,1)S(1)} %bitcast.16), channel_id=1, source_target_pairs={{0,1},{1,0},{2,3},{3,2},{4,5},{5,4},{6,7},{7,6},{8,9},{9,8},{10,11... | collective-permute-start | bytes 3145736 | tf_op jit(solution)/shard_map/ppermute | solution.py:429
  79.1 7.0 %collective-permute-start.12 = (bf16[48,2176]{1,0:T(8,128)(2,1)S(1)}, bf16[48,2176]{1,0:T(8,128)(2,1)S(1)}, u32[]{:S(2)}, u32[]{:S(2)}) collective-permute-start(bf16[48,2176]{1,0:T(8,128)(2,1)S(1)} %collective-permute-done.11.refs_2_), channel_id=1, source_target_pairs={{0,6},{1,7},{2,4},{3,5},{4,2},{5,3},{6,0},{7,1},{8,14},{9,15},{10,... | collective-permute-start | bytes 626696 | tf_op jit(solution)/shard_map/ppermute | solution.py:429
  86.1 8.3 %collective-permute-start.15 = (bf16[256,2048]{1,0:T(8,128)(2,1)S(1)}, bf16[256,2048]{1,0:T(8,128)(2,1)S(1)}, u32[]{:S(2)}, u32[]{:S(2)}) collective-permute-start(bf16[256,2048]{1,0:T(8,128)(2,1)S(1)} %bitcast.20), channel_id=1, source_target_pairs={{0,1},{1,0},{2,3},{3,2},{4,5},{5,4},{6,7},{7,6},{8,9},{9,8},{10,11... | collective-permute-start | bytes 3145736 | tf_op jit(solution)/shard_map/ppermute | solution.py:429
  93.4 2.7 %collective-permute-start.27 = (bf16[2048,256]{1,0:T(8,128)(2,1)S(1)}, bf16[2048,256]{1,0:T(8,128)(2,1)S(1)}, u32[]{:S(2)}, u32[]{:S(2)}) collective-permute-start(bf16[2048,256]{1,0:T(8,128)(2,1)S(1)} %copy-done.4), channel_id=1, source_target_pairs={{0,1},{1,0},{2,3},{3,2},{4,5},{5,4},{6,7},{7,6},{8,9},{9,8},{10,11... | collective-permute-start | bytes 3145736 | tf_op jit(solution)/shard_map/ppermute | solution.py:429
  93.4 4.1 %collective-permute-start.28 = (bf16[2048,256]{1,0:T(8,128)(2,1)S(1)}, bf16[2048,256]{1,0:T(8,128)(2,1)S(1)}, u32[]{:S(2)}, u32[]{:S(2)}) collective-permute-start(bf16[2048,256]{1,0:T(8,128)(2,1)S(1)} %copy-done.5), channel_id=1, source_target_pairs={{0,1},{1,0},{2,3},{3,2},{4,5},{5,4},{6,7},{7,6},{8,9},{9,8},{10,11... | collective-permute-start | bytes 3145736 | tf_op jit(solution)/shard_map/ppermute | solution.py:429
  93.9 5.1 %collective-permute-start.29 = (bf16[256,2048]{1,0:T(8,128)(2,1)S(1)}, bf16[256,2048]{1,0:T(8,128)(2,1)S(1)}, u32[]{:S(2)}, u32[]{:S(2)}) collective-permute-start(bf16[256,2048]{1,0:T(8,128)(2,1)S(1)} %copy-done.6), channel_id=1, source_target_pairs={{0,1},{1,0},{2,3},{3,2},{4,5},{5,4},{6,7},{7,6},{8,9},{9,8},{10,11... | collective-permute-start | bytes 3145736 | tf_op jit(solution)/shard_map/ppermute | solution.py:429
  94.0 12.5 %collective-permute-start.25 = (bf16[2048,256]{1,0:T(8,128)(2,1)S(1)}, bf16[2048,256]{1,0:T(8,128)(2,1)S(1)}, u32[]{:S(2)}, u32[]{:S(2)}) collective-permute-start(bf16[2048,256]{1,0:T(8,128)(2,1)S(1)} %collective-permute-done.19.refs_16_), channel_id=1, source_target_pairs={{0,1},{1,0},{2,3},{3,2},{4,5},{5,4},{6,7},{7,6},{8,9},{9,8},{10,11... | collective-permute-start | bytes 3145736 | tf_op jit(solution)/shard_map/ppermute | solution.py:429
  94.4 12.1 %collective-permute-start.22 = (bf16[1536,256]{1,0:T(8,128)(2,1)S(1)}, bf16[1536,256]{1,0:T(8,128)(2,1)S(1)}, u32[]{:S(2)}, u32[]{:S(2)}) collective-permute-start(bf16[1536,256]{1,0:T(8,128)(2,1)S(1)} %collective-permute-done.16.refs_10_), channel_id=1, source_target_pairs={{0,1},{1,0},{2,3},{3,2},{4,5},{5,4},{6,7},{7,6},{8,9},{9,8},{10,11... | collective-permute-start | bytes 2359304 | tf_op jit(solution)/shard_map/ppermute | solution.py:429
  96.0 9.0 %collective-permute-start.24 = (bf16[128,2048]{1,0:T(8,128)(2,1)S(1)}, bf16[128,2048]{1,0:T(8,128)(2,1)S(1)}, u32[]{:S(2)}, u32[]{:S(2)}) collective-permute-start(bf16[128,2048]{1,0:T(8,128)(2,1)S(1)} %collective-permute-done.18.refs_12_), channel_id=1, source_target_pairs={{0,1},{1,0},{2,3},{3,2},{4,5},{5,4},{6,7},{7,6},{8,9},{9,8},{10,11... | collective-permute-start | bytes 1572872 | tf_op jit(solution)/shard_map/ppermute | solution.py:429
  97.5 8.9 %collective-permute-start.26 = (bf16[128,2048]{1,0:T(8,128)(2,1)S(1)}, bf16[128,2048]{1,0:T(8,128)(2,1)S(1)}, u32[]{:S(2)}, u32[]{:S(2)}) collective-permute-start(bf16[128,2048]{1,0:T(8,128)(2,1)S(1)} %collective-permute-done.20.refs_17_), channel_id=1, source_target_pairs={{0,1},{1,0},{2,3},{3,2},{4,5},{5,4},{6,7},{7,6},{8,9},{9,8},{10,11... | collective-permute-start | bytes 1572872 | tf_op jit(solution)/shard_map/ppermute | solution.py:429
  99.0 4.5 %collective-permute-start.23 = (bf16[512,256]{1,0:T(8,128)(2,1)S(1)}, bf16[512,256]{1,0:T(8,128)(2,1)S(1)}, u32[]{:S(2)}, u32[]{:S(2)}) collective-permute-start(bf16[512,256]{1,0:T(8,128)(2,1)S(1)} %collective-permute-done.17.refs_11_), channel_id=1, source_target_pairs={{0,1},{1,0},{2,3},{3,2},{4,5},{5,4},{6,7},{7,6},{8,9},{9,8},{10,11... | collective-permute-start | bytes 786440 | tf_op jit(solution)/shard_map/ppermute | solution.py:429
  103.5 13.4 %collective-permute-start.35 = (bf16[48,2176]{1,0:T(8,128)(2,1)S(1)}, bf16[48,2176]{1,0:T(8,128)(2,1)S(1)}, u32[]{:S(2)}, u32[]{:S(2)}) collective-permute-start(bf16[48,2176]{1,0:T(8,128)(2,1)S(1)} %collective-permute-done.21.refs_2_), channel_id=1, source_target_pairs={{0,6},{1,7},{2,4},{3,5},{4,2},{5,3},{6,0},{7,1},{8,14},{9,15},{10,... | collective-permute-start | bytes 626696 | tf_op jit(solution)/shard_map/ppermute | solution.py:429
  105.0 11.9 %collective-permute-start.34 = (bf16[48,2176]{1,0:T(8,128)(2,1)S(1)}, bf16[48,2176]{1,0:T(8,128)(2,1)S(1)}, u32[]{:S(2)}, u32[]{:S(2)}) collective-permute-start(bf16[48,2176]{1,0:T(8,128)(2,1)S(1)} %collective-permute-done.33.refs_0_), channel_id=1, source_target_pairs={{0,6},{1,7},{2,4},{3,5},{4,2},{5,3},{6,0},{7,1},{8,14},{9,15},{10,... | collective-permute-start | bytes 626696 | tf_op jit(solution)/shard_map/ppermute | solution.py:429
  110.8 12.4 %collective-permute-start.30 = (bf16[48,2048]{1,0:T(8,128)(2,1)S(1)}, bf16[48,2048]{1,0:T(8,128)(2,1)S(1)}, u32[]{:S(2)}, u32[]{:S(2)}) collective-permute-start(bf16[48,2048]{1,0:T(8,128)(2,1)S(1)} %get-tuple-element.56), channel_id=1, source_target_pairs={{0,6},{1,7},{2,4},{3,5},{4,2},{5,3},{6,0},{7,1},{8,14},{9,15},{10,... | collective-permute-start | bytes 589832 | tf_op jit(solution)/shard_map/ppermute | solution.py:429
  112.3 21.7 %collective-permute-start.32 = (bf16[48,2048]{1,0:T(8,128)(2,1)S(1)}, bf16[48,2048]{1,0:T(8,128)(2,1)S(1)}, u32[]{:S(2)}, u32[]{:S(2)}) collective-permute-start(bf16[48,2048]{1,0:T(8,128)(2,1)S(1)} %get-tuple-element.58), channel_id=1, source_target_pairs={{0,6},{1,7},{2,4},{3,5},{4,2},{5,3},{6,0},{7,1},{8,14},{9,15},{10,... | collective-permute-start | bytes 589832 | tf_op jit(solution)/shard_map/ppermute | solution.py:429
  120.2 9.4 %collective-permute-start.36 = (bf16[48,2048]{1,0:T(8,128)(2,1)S(1)}, bf16[48,2048]{1,0:T(8,128)(2,1)S(1)}, u32[]{:S(2)}, u32[]{:S(2)}) collective-permute-start(bf16[48,2048]{1,0:T(8,128)(2,1)S(1)} %get-tuple-element.60), channel_id=1, source_target_pairs={{0,6},{1,7},{2,4},{3,5},{4,2},{5,3},{6,0},{7,1},{8,14},{9,15},{10,... | collective-permute-start | bytes 589832 | tf_op jit(solution)/shard_map/ppermute | solution.py:429
  121.7 11.2 %collective-permute-start.38 = (bf16[48,2048]{1,0:T(8,128)(2,1)S(1)}, bf16[48,2048]{1,0:T(8,128)(2,1)S(1)}, u32[]{:S(2)}, u32[]{:S(2)}) collective-permute-start(bf16[48,2048]{1,0:T(8,128)(2,1)S(1)} %get-tuple-element.62), channel_id=1, source_target_pairs={{0,6},{1,7},{2,4},{3,5},{4,2},{5,3},{6,0},{7,1},{8,14},{9,15},{10,... | collective-permute-start | bytes 589832 | tf_op jit(solution)/shard_map/ppermute | solution.py:429
  123.2 10.8 %collective-permute-start.31 = (bf16[48,2048]{1,0:T(8,128)(2,1)S(1)}, bf16[48,2048]{1,0:T(8,128)(2,1)S(1)}, u32[]{:S(2)}, u32[]{:S(2)}) collective-permute-start(bf16[48,2048]{1,0:T(8,128)(2,1)S(1)} %add_convert_fusion.3), channel_id=1, source_target_pairs={{0,24},{1,25},{2,26},{3,27},{4,28},{5,29},{6,30},{7,31},{8,16},{9,... | collective-permute-start | bytes 589832 | tf_op jit(solution)/shard_map/ppermute | solution.py:429
  129.6 5.7 %collective-permute-start.37 = (bf16[48,2048]{1,0:T(8,128)(2,1)S(1)}, bf16[48,2048]{1,0:T(8,128)(2,1)S(1)}, u32[]{:S(2)}, u32[]{:S(2)}) collective-permute-start(bf16[48,2048]{1,0:T(8,128)(2,1)S(1)} %add_convert_fusion.2), channel_id=1, source_target_pairs={{0,8},{1,9},{2,10},{3,11},{4,12},{5,13},{6,14},{7,15},{8,0},{9,1},... | collective-permute-start | bytes 589832 | tf_op jit(solution)/shard_map/ppermute | solution.py:429
  133.0 11.3 %collective-permute-start.39 = (bf16[48,2048]{1,0:T(8,128)(2,1)S(1)}, bf16[48,2048]{1,0:T(8,128)(2,1)S(1)}, u32[]{:S(2)}, u32[]{:S(2)}) collective-permute-start(bf16[48,2048]{1,0:T(8,128)(2,1)S(1)} %add_convert_fusion.1), channel_id=1, source_target_pairs={{0,16},{1,17},{2,18},{3,19},{4,20},{5,21},{6,22},{7,23},{8,24},{9,... | collective-permute-start | bytes 589832 | tf_op jit(solution)/shard_map/ppermute | solution.py:429
  (3 other events, 26.5 us)
